TPU v7x, 32 devices: a whole 2x2x4 slice. The times are simulated.
32 devices in a mesh: sp: 16 (over z, y, core), tp: 2 (over x).
Axes of the slice: x: 2, y: 2, z: 4, core: 2. Of those that a mesh axis runs over, the one named last changes fastest.
Arguments:
- tokens: bfloat16 [4096, 2048], P('sp', 'tp'), may hold values from -64 to 64
- input_norm_gain: float32 [2048], replicated, may hold values from 0.1 to 1.9
- attention_query_weight: bfloat16 [2048, 512], P(None, 'tp'), may hold values from -0.21875 to 0.21875
- attention_key_weight: bfloat16 [2048, 512], P(None, 'tp'), may hold values from -0.21875 to 0.21875
- attention_value_weight: bfloat16 [2048, 512], P(None, 'tp'), may hold values from -0.125 to 0.125
- attention_score_bias: float32 [8], P('tp'), may hold values from -18 to -7
- recurrence_query_weight: bfloat16 [2048, 1024], P(None, 'tp'), may hold values from -0.125 to 0.125
- forget_weight: bfloat16 [2048, 1024], P(None, 'tp'), may hold values from -0.125 to 0.125
- input_weight: bfloat16 [2048, 512], P(None, 'tp'), may hold values from -0.125 to 0.125
- output_gate_weight: bfloat16 [2048, 512], P(None, 'tp'), may hold values from -0.125 to 0.125
- forget_minimum: float32 [8, 128], P('tp'), may hold values from 0.9 to 1
- decay_spikes: float32 [4096, 8], P('sp', 'tp'), may hold values from -2.2 to 0
- head_norm_gain: float32 [64], replicated, may hold values from 0.1 to 1.9
- attention_output_weight: bfloat16 [512, 2048], P('tp'), may hold values from -0.25 to 0.25
- recurrence_output_weight: bfloat16 [512, 2048], P('tp'), may hold values from -0.25 to 0.25
Outputs:
- mixed: bfloat16 [4096, 2048], P('sp', 'tp')
All inputs are finite; a program needn't handle non-finite values.
Results may differ from a plain program's by a relative error of at most 0.018.
Values may be sent and summed in bfloat16 or wider, within the bound.
A program may use at most 64 MiB of HBM per device.

v0:
```python
import functools

import jax
import jax.numpy as jnp
from jax import lax
from jax.experimental import pallas as pl
from jax.experimental.pallas import tpu as pltpu
from jax.sharding import PartitionSpec as P

HEAD = 64
REC_KEY = 128
REC_VAL = 64
TAIL = 16
epsilon = 1e-06
VMEM = pl.BlockSpec(memory_space=pltpu.VMEM)
SMEM = pl.BlockSpec(memory_space=pltpu.SMEM)
NT = (((1,), (1,)), ((), ()))
TN = (((0,), (0,)), ((), ()))


def mm(a, b, dims=(((1,), (0,)), ((), ()))):
    return lax.dot_general(a, b, dims, preferred_element_type=jnp.float32)


def split(x):
    hi = x.astype(jnp.bfloat16)
    return hi, (x - hi.astype(jnp.float32)).astype(jnp.bfloat16)


def iota(shape, dim):
    return lax.broadcasted_iota(jnp.int32, shape, dim)


def local_kernel(
    key_ref, value_ref, q_ref, f_ref, v_ref, low_ref, spike_ref, spike_t_ref, out_ref, qdec_ref, pay_ref
):
    rows, width = key_ref.shape
    pay_ref[0:rows, :width] = key_ref[...]
    pay_ref[0:rows, width:] = value_ref[...]
    which = iota((TAIL, REC_KEY), 0)
    heads = v_ref.shape[1] // REC_VAL
    r, c = iota((rows, rows), 0), iota((rows, rows), 1)
    causal = r >= c
    lower = causal.astype(jnp.bfloat16)
    upper = (r <= c).astype(jnp.bfloat16)
    hi, lo = split(spike_ref[...])
    spike_col = mm(lower, hi) + mm(lower, lo)
    hi, lo = split(spike_t_ref[...])
    spike_row = mm(hi, upper) + mm(lo, upper)
    for h in range(heads):
        ks = slice(h * REC_KEY, (h + 1) * REC_KEY)
        vs = slice(h * REC_VAL, (h + 1) * REC_VAL)
        q = q_ref[:, ks].astype(jnp.float32)
        lifted = q * jax.nn.sigmoid(q)
        intake = (1.0 - low_ref[:, ks]) * jax.nn.sigmoid(-f_ref[:, ks].astype(jnp.float32))
        hi, lo = split(jnp.log1p(-intake))
        run = mm(lower, hi) + mm(lower, lo)
        s_col = spike_col[:, h : h + 1]
        s_row = spike_row[h : h + 1, :]
        q_up = lifted * jnp.exp(run)
        k_down = (intake * jnp.exp(-run)).astype(jnp.bfloat16)
        decay = jnp.exp(jnp.where(causal, s_col - s_row, 0.0))
        inner = jnp.where(causal, mm(q_up.astype(jnp.bfloat16), k_down, NT) * decay, 0.0)
        v = v_ref[:, vs]
        out_ref[:, vs] = mm(inner.astype(jnp.bfloat16), v)
        qdec_ref[:, ks] = (q_up * jnp.exp(s_col)).astype(jnp.bfloat16)
        total = run[rows - 1 : rows, :] + s_col[rows - 1 : rows, :]
        k_end = (intake * jnp.exp(total - (run + s_col))).astype(jnp.bfloat16)
        pay_ref[rows : rows + REC_VAL, ks] = mm(v, k_end, TN).astype(jnp.bfloat16)
        hi, lo = split(total)
        lo, rest = split(total - hi.astype(jnp.float32))
        tail = jnp.where(which == 0, hi.astype(jnp.float32), jnp.where(which == 1, lo.astype(jnp.float32), 0.0))
        tail = jnp.where(which == 2, rest.astype(jnp.float32), tail)
        pay_ref[rows + REC_VAL :, ks] = tail.astype(jnp.bfloat16)


def mix_kernel(bias_ref, q_ref, kv_ref, local_ref, qdec_ref, gate_ref, gain_ref, out_ref, acc, carry, state):
    rows, width = q_ref.shape
    heads = width // HEAD
    place = lax.axis_index("sp")
    r, c = iota((rows, rows), 0), iota((rows, rows), 1)
    before = c < r
    sums = jnp.concatenate(
        [(r > c).astype(jnp.bfloat16), jnp.ones((rows, 128), jnp.bfloat16)], axis=1
    )

    def block(number, first):
        for h in range(heads):
            hs = slice(h * HEAD, (h + 1) * HEAD)
            k = kv_ref[number, :rows, hs]
            v = kv_ref[number, :rows, width + h * HEAD : width + (h + 1) * HEAD]
            s = mm(q_ref[:, hs] * jnp.bfloat16(HEAD**-0.5), k, NT) + bias_ref[h]
            t = jnp.exp(-jnp.abs(s))
            soft = jnp.where(t < 3.5e-4, t, jnp.log(1.0 + t))
            log_sig = jnp.minimum(s, 0.0) - soft
            rest = log_sig - s
            if first:
                rest = jnp.where(before, rest, 0.0)
            both = mm(rest.astype(jnp.bfloat16), sums)
            later = both[:, :rows]
            if not first:
                later = later + jnp.concatenate([carry[h]] * (rows // 128), axis=1)
            w = jnp.exp(log_sig + later)
            if first:
                w = jnp.where(before, w, 0.0)
            o = mm(w.astype(jnp.bfloat16), v)
            if first:
                acc[:, hs] = o
                carry[h] = both[:, rows:]
            else:
                acc[:, hs] += o
                carry[h] += both[:, rows:]

    block(place, True)

    @pl.loop(0, place)
    def _(step):
        block(place - 1 - step, False)

    out_ref[:, :width] = acc[...].astype(jnp.bfloat16)

    state[...] = jnp.zeros_like(state)

    def earlier(step, suffix):
        number = place - 1 - step
        state[...] += kv_ref[number, rows : rows + REC_VAL, :].astype(jnp.float32) * jnp.exp(suffix)
        tail = kv_ref[number, rows + REC_VAL :, :].astype(jnp.float32)
        return suffix + jnp.sum(tail, axis=0, keepdims=True)

    lax.fori_loop(0, place, earlier, jnp.zeros((1, state.shape[1]), jnp.float32))
    for h in range(local_ref.shape[1] // REC_VAL):
        ks = slice(h * REC_KEY, (h + 1) * REC_KEY)
        vs = slice(h * REC_VAL, (h + 1) * REC_VAL)
        raw = local_ref[:, vs] + mm(qdec_ref[:, ks], state[:, ks].astype(jnp.bfloat16), NT)
        gate = gate_ref[:, vs].astype(jnp.float32)
        mean = jnp.sum(raw * raw, axis=1, keepdims=True) * (1.0 / REC_VAL)
        done = raw * lax.rsqrt(mean + epsilon) * gain_ref[...] * (gate * jax.nn.sigmoid(gate))
        out_ref[:, width + h * REC_VAL : width + (h + 1) * REC_VAL] = done.astype(jnp.bfloat16)


def gather_kernel(planes, in_ref, out_ref, own_sem, send_sem, recv_sem):
    me = lax.axis_index("sp")
    c, y, z = lax.rem(me, 2), lax.rem(me // 2, 2), me // 4
    across, other = z * 4 + (1 - y) * 2 + c, z * 4 + y * 2 + (1 - c)
    ahead = lax.rem(z + 1, planes) * 4 + y * 2 + c
    behind = lax.rem(z + planes - 1, planes) * 4 + y * 2 + c
    barrier = pltpu.get_barrier_semaphore()
    for neighbour in (across, other, ahead, behind):
        pl.semaphore_signal(barrier, inc=1, device_id={"sp": neighbour}, device_id_type=pl.DeviceIdType.MESH)
    own = pltpu.make_async_copy(in_ref, out_ref.at[me], own_sem)
    own.start()
    pl.semaphore_wait(barrier, 4)
    own.wait()

    def copy(number, way, target):
        return pltpu.make_async_remote_copy(
            src_ref=out_ref.at[number],
            dst_ref=out_ref.at[number],
            send_sem=send_sem.at[way, number],
            recv_sem=recv_sem.at[number],
            device_id={"sp": target},
            device_id_type=pl.DeviceIdType.MESH,
        )

    def column(d):
        return (z - d) * 4 + y * 2 + c

    def facing(d):
        return (z - d) * 4 + (1 - y) * 2 + c

    def column_sends(d, act):
        @pl.when(z < planes - 1)
        def _():
            act(copy(column(d), 0, ahead))

        @pl.when((d > 0) | (y == 0))
        def _():
            act(copy(column(d), 1, across))

        @pl.when((d > 0) | (c == 0))
        def _():
            act(copy(column(d), 2, other))

    def facing_sends(d, act):
        @pl.when((d > 0) | (y == 1))
        def _():
            act(copy(facing(d), 2, other))

    def start(one):
        one.start()

    @pl.loop(0, z + 2)
    def _(d):
        @pl.when(d <= z)
        def _():
            @pl.when(d > 0)
            def _():
                copy(column(d), 0, ahead).wait_recv()

            column_sends(d, start)

        @pl.when(d > 0)
        def _():
            @pl.when((d > 1) | (y == 1))
            def _():
                copy(facing(d - 1), 1, across).wait_recv()

            facing_sends(d - 1, start)

    @pl.loop(0, z + 1)
    def _(d):
        @pl.when((d > 0) | (c == 1))
        def _():
            copy((z - d) * 4 + y * 2 + 1 - c, 2, other).wait_recv()

        @pl.when((d > 0) | (y == 1))
        def _():
            copy((z - d) * 4 + (1 - y) * 2 + 1 - c, 2, other).wait_recv()

        column_sends(d, lambda one: one.wait_send())
        facing_sends(d, lambda one: one.wait_send())


def shards(
    sp,
    tp,
    tokens,
    input_norm_gain,
    attention_query_weight,
    attention_key_weight,
    attention_value_weight,
    attention_score_bias,
    recurrence_query_weight,
    forget_weight,
    input_weight,
    output_gate_weight,
    forget_minimum,
    decay_spikes,
    head_norm_gain,
    attention_output_weight,
    recurrence_output_weight,
):
    rows = tokens.shape[0]
    mine = lax.axis_index("tp")

    def to_partner(array, shift):
        return lax.ppermute(array, "tp", [(i, (i + shift) % tp) for i in range(tp)])

    features = tokens.shape[1]
    pieces = [tokens] + [to_partner(tokens, shift) for shift in range(1, tp)]
    attention_output_weight, recurrence_output_weight, pieces[-1] = lax.optimization_barrier(
        (attention_output_weight, recurrence_output_weight, pieces[-1])
    )
    own_rows = jnp.concatenate([attention_output_weight, recurrence_output_weight], axis=0)
    columns = own_rows.shape[1] // tp

    def cut(shift):
        return lax.dynamic_slice_in_dim(own_rows, lax.rem(mine + shift, tp) * columns, columns, 1)

    out_weights = [cut(0)] + [to_partner(cut(shift), shift) for shift in range(1, tp)]

    starts = [lax.rem(mine + tp - shift, tp) * features for shift in range(tp)]
    values = [piece.astype(jnp.float32) for piece in pieces]
    scaled = [
        (value * lax.dynamic_slice_in_dim(input_norm_gain, start, features, 0)[None, :]).astype(jnp.bfloat16)
        for value, start in zip(values, starts)
    ]
    squares = sum(jnp.sum(value * value, axis=1) for value in values) / (features * tp)
    inverse = lax.rsqrt(squares + epsilon)[:, None]

    def project(weight):
        total = sum(
            jnp.dot(part, lax.dynamic_slice_in_dim(weight, start, features, 0), preferred_element_type=jnp.float32)
            for part, start in zip(scaled, starts)
        )
        return (total * inverse).astype(jnp.bfloat16)

    key_stick, value_stick = project(attention_key_weight), project(attention_value_weight)
    query_rows, forget_rows = project(recurrence_query_weight), project(forget_weight)
    input_rows = project(input_weight)
    heads_here = forget_minimum.shape[0]
    wide, narrow = heads_here * REC_KEY, heads_here * REC_VAL
    local_out, query_decayed, payload = pl.pallas_call(
        local_kernel,
        out_shape=(
            jax.ShapeDtypeStruct((rows, narrow), jnp.float32),
            jax.ShapeDtypeStruct((rows, wide), jnp.bfloat16),
            jax.ShapeDtypeStruct((rows + REC_VAL + TAIL, wide), jnp.bfloat16),
        ),
        in_specs=[VMEM] * 8,
        out_specs=(VMEM,) * 3,
        cost_estimate=pl.CostEstimate(flops=10**9, bytes_accessed=2 * 10**6, transcendentals=10**6),
        name="recurrence_local",
    )(
        key_stick,
        value_stick,
        query_rows,
        forget_rows,
        input_rows,
        forget_minimum.reshape(1, wide),
        decay_spikes,
        decay_spikes.T,
    )
    kv_all = pl.pallas_call(
        functools.partial(gather_kernel, sp // 4),
        out_shape=jax.ShapeDtypeStruct((sp,) + payload.shape, payload.dtype),
        in_specs=[VMEM],
        out_specs=VMEM,
        scratch_shapes=[
            pltpu.SemaphoreType.DMA,
            pltpu.SemaphoreType.DMA((3, sp)),
            pltpu.SemaphoreType.DMA((sp,)),
        ],
        compiler_params=pltpu.CompilerParams(collective_id=0, has_side_effects=True),
        cost_estimate=pl.CostEstimate(flops=10**10, bytes_accessed=10**8, transcendentals=0),
        name="gather_earlier",
    )(payload)
    query_stick, gate_rows = project(attention_query_weight), project(output_gate_weight)
    width = query_stick.shape[1]
    heads = pl.pallas_call(
        mix_kernel,
        out_shape=jax.ShapeDtypeStruct((rows, width + narrow), jnp.bfloat16),
        in_specs=[SMEM] + [VMEM] * 6,
        out_specs=VMEM,
        scratch_shapes=[
            pltpu.VMEM((rows, width), jnp.float32),
            pltpu.VMEM((width // HEAD, rows, 128), jnp.float32),
            pltpu.VMEM((REC_VAL, wide), jnp.float32),
        ],
        compiler_params=pltpu.CompilerParams(vmem_limit_bytes=60 * 1024 * 1024),
        name="mix_heads",
    )(
        attention_score_bias,
        query_stick,
        kv_all,
        local_out,
        query_decayed,
        gate_rows,
        head_norm_gain.reshape(1, REC_VAL),
    )
    mixed = jnp.dot(heads, out_weights[0], preferred_element_type=jnp.float32)
    for shift in range(1, tp):
        mixed = mixed + jnp.dot(to_partner(heads, shift), out_weights[shift], preferred_element_type=jnp.float32)
    return mixed.astype(jnp.bfloat16)


def solution(mesh):
    placed = (
        P("sp", "tp"),
        P(),
        P(None, "tp"),
        P(None, "tp"),
        P(None, "tp"),
        P("tp"),
        P(None, "tp"),
        P(None, "tp"),
        P(None, "tp"),
        P(None, "tp"),
        P("tp", None),
        P("sp", "tp"),
        P(),
        P("tp", None),
        P("tp", None),
    )
    return jax.shard_map(
        functools.partial(shards, mesh.shape["sp"], mesh.shape["tp"]),
        mesh=mesh,
        in_specs=placed,
        out_specs=P("sp", "tp"),
        check_vma=False,
    )
```

profile of v0, /device:TPU:29, one launch (start us, length us, event | category | flops | bytes accessed | tf_op | source)
XLA Modules:
  0.0 103.1 jit_solution(15564405540854462081)
XLA Ops:
  0.0 1.2 %collective-permute-start = (bf16[256,1024]{1,0:T(8,128)(2,1)}, bf16[256,1024]{1,0:T(8,128)(2,1)S(1)}, u32[]{:S(2)}, u32[]{:S(2)}) collective-permute-start(bf16[256,1024]{1,0:T(8,128)(2,1)} %param.15), channel_id=1, source_target_pairs={{0,1},{1,0},{2,3},{3,2},{4,5},{5,4},{6,7},{7,6},{8,9},{9,8},{10,11... | collective-permute-start | bytes 1572872 | tf_op jit(solution)/shard_map/ppermute | solution.py:247
  1.2 0.9 fusion.71
  2.1 2.2 %fusion.31 = f32[256,256]{1,0:T(8,128)} fusion(bf16[2048,256]{1,0:T(8,128)(2,1)} %param.23, s32[]{:T(128)S(6)} %select_n.6, bf16[256,1024]{1,0:T(8,128)(2,1)} %param.15, f32[1024]{0:T(1024)S(1)} %get-tuple-element.18), kind=kOutput, calls=%fused_computation.43 | convolution fusion | flops 135004160 | bytes 1314820 | tf_op jit(solution)/shard_map/dot_general | solution.py:273
  4.3 2.3 %fusion.34 = f32[256,256]{1,0:T(8,128)} fusion(bf16[2048,256]{1,0:T(8,128)(2,1)} %param.19, s32[]{:T(128)S(6)} %select_n.6, bf16[256,1024]{1,0:T(8,128)(2,1)} %param.15, f32[1024]{0:T(1024)S(1)} %get-tuple-element.18), kind=kOutput, calls=%fused_computation.46 | convolution fusion | flops 135004160 | bytes 1314820 | tf_op jit(solution)/shard_map/dot_general | solution.py:273
  6.6 1.0 fusion.37
  7.6 1.0 fusion.28
  9.2 0.8 copy.16.spike_ref
  10.4 1.1 %copy-done.3 = bf16[2048,512]{1,0:T(8,128)(2,1)S(1)} copy-done((bf16[2048,512]{1,0:T(8,128)(2,1)S(1)}, bf16[2048,512]{1,0:T(8,128)(2,1)}, u32[]{:S(2)}) %copy-start.3) | copy-done | bytes 2097176
  12.0 1.0 collective-permute-done
  13.2 1.2 %fusion.3.f_ref = bf16[256,512]{1,0:T(8,128)(2,1)} fusion(f32[256,512]{1,0:T(8,128)S(1)} %fusion.22, bf16[2048,512]{1,0:T(8,128)(2,1)S(1)} %copy-done, s32[]{:T(128)S(6)} %select_n.7, f32[256]{0:T(256)S(1)} %add_rsqrt_fusion, bf16[256,1024]{1,0:T(8,128)(2,1)S(1)} %collective-permute-done, f32[1024]{0:T(1024)S(1)} %get-tuple-element.17), kind=kOutput, calls=%fused_computation.10 | convolution fusion | flops 269615104 | bytes 2364420 | tf_op jit(solution)/shard_map/dot_general | solution.py:273
  14.4 1.2 %fusion.4.q_ref = bf16[256,512]{1,0:T(8,128)(2,1)} fusion(f32[256,512]{1,0:T(8,128)S(1)} %fusion.25, bf16[2048,512]{1,0:T(8,128)(2,1)S(1)} %copy-done.3, s32[]{:T(128)S(6)} %select_n.7, f32[256]{0:T(256)S(1)} %add_rsqrt_fusion, bf16[256,1024]{1,0:T(8,128)(2,1)S(1)} %collective-permute-done, f32[1024]{0:T(1024)S(1)} %get-tuple-element.17), kind=kOutput, calls=%fused_computation.11 | convolution fusion | flops 269615104 | bytes 2364420 | tf_op jit(solution)/shard_map/dot_general | solution.py:273
  15.6 1.0 fusion.11.v_ref
  16.6 1.0 fusion.12.value_ref
  17.6 1.0 fusion.13.key_ref
  18.5 1.0 fusion.10.gate_ref
  19.5 1.0 fusion.14.q_ref
  20.9 1.3 %copy-done.2 = bf16[512,2048]{1,0:T(8,128)(2,1)} copy-done((bf16[512,2048]{1,0:T(8,128)(2,1)}, bf16[512,2048]{1,0:T(8,128)(2,1)S(1)}, u32[]{:S(2)}) %copy-start.2) | copy-done | bytes 2097176
  22.3 1.3 %collective-permute-start.2 = (bf16[512,1024]{1,0:T(8,128)(2,1)S(1)}, bf16[512,1024]{1,0:T(8,128)(2,1)}, u32[]{:S(2)}, u32[]{:S(2)}) collective-permute-start(bf16[512,1024]{1,0:T(8,128)(2,1)S(1)} %constant_dynamic-slice_fusion), channel_id=1, source_target_pairs={{0,1},{1,0},{2,3},{3,2},{4,5},{5,4},{6,7},{7,6},{8,9},{9,8},{10,11... | collective-permute-start | bytes 3145736 | tf_op jit(solution)/shard_map/ppermute | solution.py:247
  23.6 4.2 %recurrence_local.1 = (f32[256,256]{1,0:T(8,128)}, bf16[256,512]{1,0:T(8,128)(2,1)}, bf16[336,512]{1,0:T(8,128)(2,1)}) custom-call(bf16[256,256]{1,0:T(8,128)(2,1)} %fusion.13.key_ref, bf16[256,256]{1,0:T(8,128)(2,1)} %fusion.12.value_ref, bf16[256,512]{1,0:T(8,128)(2,1)} %fusion.4.q_ref, bf16[256,512]{1,0:T(8,128)(2,1)} %fusion.3.f_ref, ...), custom_call_target="tpu_custom_call" | custom-call | flops 1000000000 | bytes 2000000 | tf_op jit(solution)/shard_map/recurrence_local/pallas_call | solution.py:283
  27.7 38.3 %gather_earlier.1.kv_ref = bf16[16,336,512]{2,1,0:T(8,128)(2,1)} custom-call(bf16[336,512]{1,0:T(8,128)(2,1)} %get-tuple-element.12.in_ref), custom_call_target="tpu_custom_call" | custom-call | flops 10000000000 | bytes 100000000 | tf_op jit(solution)/shard_map/gather_earlier/pallas_call | solution.py:304
  66.1 27.2 %mix_heads.1 = bf16[256,512]{1,0:T(8,128)(2,1)} custom-call(f32[4]{0:T(128)} %bias_ref.1, bf16[256,256]{1,0:T(8,128)(2,1)} %fusion.14.q_ref, bf16[16,336,512]{2,1,0:T(8,128)(2,1)} %gather_earlier.1.kv_ref, f32[256,256]{1,0:T(8,128)} %get-tuple-element.13.local_ref, bf16[256,512]{1,0:T(8,128)(2,1)} %get-tuple-element.14.qdec_ref, ...), custom_call_target="tpu_custom_call" | custom-call | tf_op jit(solution)/shard_map/mix_heads/pallas_call | solution.py:320
  93.5 1.7 %fusion.19 = f32[256,1024]{1,0:T(8,128)S(1)} fusion(bf16[256,512]{1,0:T(8,128)(2,1)} %mix_heads.1, bf16[512,2048]{1,0:T(8,128)(2,1)} %copy-done.2, s32[]{:T(128)S(6)} %select_n.8), kind=kOutput, calls=%fused_computation.31 | convolution fusion | flops 268435456 | bytes 2359300 | tf_op jit(solution)/shard_map/dot_general | solution.py:341
  95.2 5.4 %collective-permute-done.1 = bf16[256,512]{1,0:T(8,128)(2,1)S(1)} collective-permute-done((bf16[256,512]{1,0:T(8,128)(2,1)}, bf16[256,512]{1,0:T(8,128)(2,1)S(1)}, u32[]{:S(2)}, u32[]{:S(2)}) %collective-permute-start.1) | collective-permute-done | bytes 262176 | tf_op jit(solution)/shard_map/ppermute | solution.py:247
  100.6 2.5 %fusion = bf16[256,1024]{1,0:T(8,128)(2,1)} fusion(f32[256,1024]{1,0:T(8,128)S(1)} %fusion.19, bf16[256,512]{1,0:T(8,128)(2,1)S(1)} %collective-permute-done.1, bf16[512,1024]{1,0:T(8,128)(2,1)} %collective-permute-done.2), kind=kOutput, calls=%fused_computation.5 | convolution fusion | flops 268959744 | bytes 2883584 | tf_op jit(solution)/shard_map/dot_general | solution.py:343
  (47 shorter events, 2.3 us)
Async XLA Ops:
  0.0 10.0 %copy-start = (bf16[2048,512]{1,0:T(8,128)(2,1)S(1)}, bf16[2048,512]{1,0:T(8,128)(2,1)}, u32[]{:S(2)}) copy-start(bf16[2048,512]{1,0:T(8,128)(2,1)} %param.22) | copy-start | bytes 6291460
  0.0 6.6 %copy-start.1 = (bf16[256,1024]{1,0:T(8,128)(2,1)S(1)}, bf16[256,1024]{1,0:T(8,128)(2,1)}, u32[]{:S(2)}) copy-start(bf16[256,1024]{1,0:T(8,128)(2,1)} %param.15) | copy-start | bytes 1572868
  0.0 13.0 %collective-permute-start = (bf16[256,1024]{1,0:T(8,128)(2,1)}, bf16[256,1024]{1,0:T(8,128)(2,1)S(1)}, u32[]{:S(2)}, u32[]{:S(2)}) collective-permute-start(bf16[256,1024]{1,0:T(8,128)(2,1)} %param.15), channel_id=1, source_target_pairs={{0,1},{1,0},{2,3},{3,2},{4,5},{5,4},{6,7},{7,6},{8,9},{9,8},{10,11... | collective-permute-start | bytes 1572872 | tf_op jit(solution)/shard_map/ppermute | solution.py:247
  1.2 5.4 %copy-start.8 = (bf16[2048,256]{1,0:T(8,128)(2,1)S(1)}, bf16[2048,256]{1,0:T(8,128)(2,1)}, u32[]{:S(2)}) copy-start(bf16[2048,256]{1,0:T(8,128)(2,1)} %param.18) | copy-start | bytes 3145732
  1.2 6.4 %copy-start.10 = (bf16[2048,256]{1,0:T(8,128)(2,1)S(1)}, bf16[2048,256]{1,0:T(8,128)(2,1)}, u32[]{:S(2)}) copy-start(bf16[2048,256]{1,0:T(8,128)(2,1)} %param.24) | copy-start | bytes 3145732
  4.3 4.4 %copy-start.12 = (bf16[2048,256]{1,0:T(8,128)(2,1)S(1)}, bf16[2048,256]{1,0:T(8,128)(2,1)}, u32[]{:S(2)}) copy-start(bf16[2048,256]{1,0:T(8,128)(2,1)} %param.17) | copy-start | bytes 3145732
  6.6 2.6 %copy-start.18 = (f32[256,4]{0,1:T(4,128)S(1)}, f32[256,4]{0,1:T(4,128)}, u32[]{:S(2)}) copy-start(f32[256,4]{0,1:T(4,128)} %param.26) | copy-start | bytes 12292
  10.0 1.6 %copy-start.3 = (bf16[2048,512]{1,0:T(8,128)(2,1)S(1)}, bf16[2048,512]{1,0:T(8,128)(2,1)}, u32[]{:S(2)}) copy-start(bf16[2048,512]{1,0:T(8,128)(2,1)} %param.21) | copy-start | bytes 6291460
  13.2 2.4 %copy-start.6 = (bf16[2048,256]{1,0:T(8,128)(2,1)S(1)}, bf16[2048,256]{1,0:T(8,128)(2,1)}, u32[]{:S(2)}) copy-start(bf16[2048,256]{1,0:T(8,128)(2,1)} %param.23) | copy-start | bytes 3145732
  13.2 2.4 %copy-start.17 = (f32[256,256]{1,0:T(8,128)S(1)}, f32[256,256]{1,0:T(8,128)}, u32[]{:S(2)}) copy-start(f32[256,256]{1,0:T(8,128)} %fusion.31) | copy-start | bytes 786436
  14.4 2.2 %copy-start.7 = (bf16[2048,256]{1,0:T(8,128)(2,1)S(1)}, bf16[2048,256]{1,0:T(8,128)(2,1)}, u32[]{:S(2)}) copy-start(bf16[2048,256]{1,0:T(8,128)(2,1)} %param.19) | copy-start | bytes 3145732
  14.4 2.2 %copy-start.16 = (f32[256,256]{1,0:T(8,128)S(1)}, f32[256,256]{1,0:T(8,128)}, u32[]{:S(2)}) copy-start(f32[256,256]{1,0:T(8,128)} %fusion.34) | copy-start | bytes 786436
  14.4 3.2 %copy-start.9 = (bf16[2048,256]{1,0:T(8,128)(2,1)S(1)}, bf16[2048,256]{1,0:T(8,128)(2,1)}, u32[]{:S(2)}) copy-start(bf16[2048,256]{1,0:T(8,128)(2,1)} %param.18) | copy-start | bytes 3145732
  14.4 3.2 %copy-start.15 = (f32[256,256]{1,0:T(8,128)S(1)}, f32[256,256]{1,0:T(8,128)}, u32[]{:S(2)}) copy-start(f32[256,256]{1,0:T(8,128)} %fusion.37) | copy-start | bytes 786436
  15.6 2.9 %copy-start.11 = (bf16[2048,256]{1,0:T(8,128)(2,1)S(1)}, bf16[2048,256]{1,0:T(8,128)(2,1)}, u32[]{:S(2)}) copy-start(bf16[2048,256]{1,0:T(8,128)(2,1)} %param.24) | copy-start | bytes 3145732
  15.6 2.9 %copy-start.14 = (f32[256,256]{1,0:T(8,128)S(1)}, f32[256,256]{1,0:T(8,128)}, u32[]{:S(2)}) copy-start(f32[256,256]{1,0:T(8,128)} %fusion.28) | copy-start | bytes 786436
  16.6 2.9 %copy-start.13 = (bf16[2048,256]{1,0:T(8,128)(2,1)S(1)}, bf16[2048,256]{1,0:T(8,128)(2,1)}, u32[]{:S(2)}) copy-start(bf16[2048,256]{1,0:T(8,128)(2,1)} %param.17) | copy-start | bytes 3145732
  17.6 2.9 %copy-start.4 = (bf16[256,2048]{1,0:T(8,128)(2,1)S(1)}, bf16[256,2048]{1,0:T(8,128)(2,1)}, u32[]{:S(2)}) copy-start(bf16[256,2048]{1,0:T(8,128)(2,1)} %param.28) | copy-start | bytes 3145732
  19.5 1.2 %copy-start.5 = (bf16[256,2048]{1,0:T(8,128)(2,1)S(1)}, bf16[256,2048]{1,0:T(8,128)(2,1)}, u32[]{:S(2)}) copy-start(bf16[256,2048]{1,0:T(8,128)(2,1)} %param.29) | copy-start | bytes 3145732
  20.9 1.3 %copy-start.2 = (bf16[512,2048]{1,0:T(8,128)(2,1)}, bf16[512,2048]{1,0:T(8,128)(2,1)S(1)}, u32[]{:S(2)}) copy-start(bf16[512,2048]{1,0:T(8,128)(2,1)S(1)} %constant_dynamic-update-slice_fusion) | copy-start | bytes 6291460
  22.3 78.4 %collective-permute-start.2 = (bf16[512,1024]{1,0:T(8,128)(2,1)S(1)}, bf16[512,1024]{1,0:T(8,128)(2,1)}, u32[]{:S(2)}, u32[]{:S(2)}) collective-permute-start(bf16[512,1024]{1,0:T(8,128)(2,1)S(1)} %constant_dynamic-slice_fusion), channel_id=1, source_target_pairs={{0,1},{1,0},{2,3},{3,2},{4,5},{5,4},{6,7},{7,6},{8,9},{9,8},{10,11... | collective-permute-start | bytes 3145736 | tf_op jit(solution)/shard_map/ppermute | solution.py:247
  93.2 7.4 %collective-permute-start.1 = (bf16[256,512]{1,0:T(8,128)(2,1)}, bf16[256,512]{1,0:T(8,128)(2,1)S(1)}, u32[]{:S(2)}, u32[]{:S(2)}) collective-permute-start(bf16[256,512]{1,0:T(8,128)(2,1)} %mix_heads.1), channel_id=1, source_target_pairs={{0,1},{1,0},{2,3},{3,2},{4,5},{5,4},{6,7},{7,6},{8,9},{9,8},{10,11... | collective-permute-start | bytes 786440 | tf_op jit(solution)/shard_map/ppermute | solution.py:247
where the time goes:
time: 103 us
  Pallas kernels  69.7 us (68%)
  matrix products  19.2 us (19%)
  waiting for transfers between devices  6.41 us (6%)
  local copies, waits for them, and re-layouts  4.59 us (4%)
  starting transfers between devices  2.73 us (3%)
    pallas_call x1, Pallas kernels, shards(): pl.pallas_call(functools.partial(gather_kernel, sp // 4), out_shape=jax.S...  38.3 us
    pallas_call x1, Pallas kernels, shards(): pl.pallas_call(mix_kernel, out_shape=jax.ShapeDtypeStruct((rows, width +...  27.2 us
    dot_general x14, matrix products, project(): jnp.dot(part, lax.dynamic_slice_in_dim(weight, start, features, 0), prefe...  15 us
    ppermute x3, waiting for transfers between devices, to_partner(): return lax.ppermute(array, 'tp', [(i, (i + shift) % tp) for i in range(tp)])  6.41 us
    pallas_call x1, Pallas kernels, shards(): pl.pallas_call(local_kernel, out_shape=(jax.ShapeDtypeStruct((rows, narro...  4.18 us
    unnamed x40, local copies, waits for them, and re-layouts  3.55 us
    ppermute x3, starting transfers between devices, to_partner(): return lax.ppermute(array, 'tp', [(i, (i + shift) % tp) for i in range(tp)])  2.73 us
    dot_general x1, matrix products, shards(): jnp.dot(to_partner(heads, shift), out_weights[shift], preferred_element_t...  2.46 us
  transfers between devices with their start and end apart: 3, of which 2 were waited for; matrix products, arithmetic and copies ran while one was open for 11% of the time, Pallas kernels for 68%

commit v1 on v0

v1 whole, which is shorter than its diff:
```python
import functools
import math
import types

import jax
import jax.numpy as jnp
from jax import lax
from jax.experimental import pallas as pl
from jax.experimental.pallas import tpu as pltpu
from jax.sharding import PartitionSpec as P

HEAD = 64
REC_KEY = 128
REC_VAL = 64
LANES = 128
GROUP = 4
TAIL = 16
LOG2E = math.log2(math.e)
epsilon = 1e-06
VMEM = pl.BlockSpec(memory_space=pltpu.VMEM)
SMEM = pl.BlockSpec(memory_space=pltpu.SMEM)
ANY = pl.BlockSpec(memory_space=pl.ANY)
NT = (((1,), (1,)), ((), ()))
TN = (((0,), (0,)), ((), ()))


def mm(a, b, dims=(((1,), (0,)), ((), ()))):
    return lax.dot_general(a, b, dims, preferred_element_type=jnp.float32)


def split(x):
    hi = x.astype(jnp.bfloat16)
    return hi, (x - hi.astype(jnp.float32)).astype(jnp.bfloat16)


def iota(shape, dim):
    return lax.broadcasted_iota(jnp.int32, shape, dim)


def start(copies):
    for one in copies:
        one.start()


def sent(copies):
    for one in copies:
        one.wait_send()


def remote(src, dst, send_sem, recv_sem, **target):
    return pltpu.make_async_remote_copy(
        src_ref=src,
        dst_ref=dst,
        send_sem=send_sem,
        recv_sem=recv_sem,
        device_id=target,
        device_id_type=pl.DeviceIdType.MESH,
    )


def tail_of(total):
    hi, lo = split(total)
    lo, rest = split(total - hi.astype(jnp.float32))
    which = iota((TAIL, total.shape[1]), 0)
    tail = jnp.where(which == 0, hi.astype(jnp.float32), jnp.where(which == 1, lo.astype(jnp.float32), 0.0))
    return jnp.where(which == 2, rest.astype(jnp.float32), tail).astype(jnp.bfloat16)


def layer_kernel(sp, tp, names, *refs):
    m = types.SimpleNamespace(**dict(zip(names, refs)))
    rows, features = m.tok.shape[1:]
    width, wide, narrow = m.wk.shape[1], m.wr.shape[1], m.wi.shape[1]
    heads, rec_heads = width // HEAD, narrow // REC_VAL
    chunks, chunk = m.kv.shape[1], m.kv.shape[3]
    planes = sp // GROUP
    half = planes // 2
    columns = m.out.shape[1]
    span = REC_VAL // GROUP
    me, t = lax.axis_index("sp"), lax.axis_index("tp")
    c, y, z = lax.rem(me, 2), lax.rem(me // 2, 2), me // GROUP
    g = lax.rem(me, GROUP)
    sibling, across = me + 1 - 2 * c, z * GROUP + (1 - y) * 2 + c
    ahead = lax.rem(z + 1, planes) * GROUP + g
    behind = lax.rem(z + planes - 1, planes) * GROUP + g

    def mate(off):
        return z * GROUP + lax.rem(g + off, GROUP)

    def partner(shift):
        return lax.rem(t + shift, tp)

    load_tokens = pltpu.make_async_copy(m.tokens, m.tok.at[t], m.load_sem.at[0])
    load_tokens.start()
    order = "krfivqg"
    loads = [
        pltpu.make_async_copy(getattr(m, "hbm_" + name), getattr(m, "w" + name), m.load_sem.at[1 + i])
        for i, name in enumerate(order)
    ]
    start(loads)
    own_columns = pl.ds(pl.multiple_of(t * columns, columns), columns)
    outer = (m.hbm_attention_out, m.hbm_recurrence_out)
    load_outer = [
        pltpu.make_async_copy(array.at[:, own_columns], m.win.at[t, i], m.load_sem.at[8 + i])
        for i, array in enumerate(outer)
    ]
    start(load_outer)

    barrier = pltpu.get_barrier_semaphore()
    for off in range(1, GROUP):
        pl.semaphore_signal(barrier, inc=1, device_id={"sp": mate(off)}, device_id_type=pl.DeviceIdType.MESH)
    for off in range(1, planes):
        peer = lax.rem(z + off, planes) * GROUP + g
        pl.semaphore_signal(barrier, inc=1, device_id={"sp": peer}, device_id_type=pl.DeviceIdType.MESH)
    for shift in range(1, tp):
        pl.semaphore_signal(barrier, inc=1, device_id={"tp": partner(shift)}, device_id_type=pl.DeviceIdType.MESH)
    pl.semaphore_wait(barrier, GROUP + planes + tp - 3)
    load_tokens.wait()

    def token_copy(shift, r, slot):
        part = m.tok.at[slot, pl.ds(r * chunk, chunk)]
        return remote(part, part, m.tok_send.at[shift, r], m.tok_recv.at[shift, r], tp=partner(shift))

    token_sends = [token_copy(shift, r, t) for shift in range(1, tp) for r in range(chunks)]
    start(token_sends)

    def scale(slot, part):
        value = m.tok[slot, part, :].astype(jnp.float32)
        gains = m.gain[:, pl.ds(pl.multiple_of(slot * features, features), features)]
        return (value * gains).astype(jnp.bfloat16), jnp.sum(value * value, axis=1, keepdims=True)

    def weight_rows(name, slot, cut):
        return getattr(m, "w" + name)[pl.ds(pl.multiple_of(slot * features, features), features), cut]

    def tiles(name):
        size = getattr(m, "w" + name).shape[1]
        step = min(256, size)
        return [slice(i, i + step) for i in range(0, size, step)]

    scaled, squares = scale(t, slice(0, rows))
    m.own_scaled[...] = scaled
    m.square[...] = jnp.broadcast_to(squares, m.square.shape)
    for load, name in zip(loads, order):
        load.wait()
        for cut in tiles(name):
            getattr(m, "a" + name)[:, cut] = mm(m.own_scaled[...], weight_rows(name, t, cut))

    def kv_copy(number, r, way, target):
        piece = m.kv.at[number, r]
        return remote(piece, piece, m.kv_send.at[way, number, r], m.kv_recv.at[number, r], sp=target)

    def relay(zs, ys, r, act):
        number = zs * GROUP + ys * 2 + c
        column, first = ys == y, zs == 0
        here = zs == z

        @pl.when((first & (z + 1 < half)) | (~first & column & (z < planes - 1)))
        def _():
            act(kv_copy(number, r, 0, ahead))

        @pl.when(column & ((here & ((y == 0) | (z == 0))) | (~here & ~first)))
        def _():
            act(kv_copy(number, r, 1, across))

        @pl.when(first & ((z == 0) | (z > half)))
        def _():
            act(kv_copy(number, r, 2, behind))

        @pl.when(~here | (column & (c == 0)) | (~column & (y == 1)))
        def _():
            act(kv_copy(number, r, 3, sibling))

    def event(zs, ys):
        for r in range(chunks):
            kv_copy(zs * GROUP + ys * 2 + c, r, 0, ahead).wait_recv()
            relay(zs, ys, r, lambda one: one.start())

    def from_sibling(zs, ys):
        for r in range(chunks):
            kv_copy(zs * GROUP + ys * 2 + 1 - c, r, 3, sibling).wait_recv()

    for shift in range(1, tp):
        slot = lax.rem(t + tp - shift, tp)
        for r in range(chunks):
            part = slice(r * chunk, (r + 1) * chunk)
            token_copy(shift, r, slot).wait_recv()
            scaled, squares = scale(slot, part)
            m.far_scaled[part] = scaled
            m.square[part] += jnp.broadcast_to(squares, (chunk, LANES))
            if shift == tp - 1:
                inverse = lax.rsqrt(m.square[part, 0:1] * (1.0 / (features * tp)) + epsilon)
                for i, name in enumerate("kv"):
                    whole = getattr(m, "a" + name)[part, :] + mm(
                        m.far_scaled[part], weight_rows(name, slot, slice(0, width))
                    )
                    m.kv[me, r, i * width : (i + 1) * width, :] = (whole * inverse).T.astype(jnp.bfloat16)
                relay(z, y, r, lambda one: one.start())
        if shift < tp - 1:
            for name in order:
                for cut in tiles(name):
                    getattr(m, "a" + name)[:, cut] += mm(m.far_scaled[...], weight_rows(name, slot, cut))
    slot = lax.rem(t + 1, tp)

    def outer_copy(shift, array, other):
        from_columns = array.at[:, pl.ds(pl.multiple_of(partner(shift) * columns, columns), columns)]
        return remote(
            from_columns, m.win.at[t, other], m.outer_send.at[shift, 0], m.outer_recv.at[shift, 0], tp=partner(shift)
        )

    for which, array in enumerate(outer):

        @pl.when(c == which)
        def _():
            start([outer_copy(shift, array, which) for shift in range(1, tp)])

    def outer_share(shift):
        piece = m.win.at[lax.rem(t + tp - shift, tp), c]
        return remote(piece, piece, m.outer_send.at[shift, 1], m.outer_recv.at[shift, 1], sp=sibling)

    inverse = lax.rsqrt(m.square[:, 0:1] * (1.0 / (features * tp)) + epsilon)

    def project(name, cut):
        whole = getattr(m, "a" + name)[:, cut] + mm(m.far_scaled[...], weight_rows(name, slot, cut))
        return (whole * inverse).astype(jnp.bfloat16)

    for name in "rfi":
        for cut in tiles(name):
            getattr(m, "p" + name)[:, cut] = project(name, cut)

    r_iota, c_iota = iota((rows, rows), 0), iota((rows, rows), 1)
    causal = r_iota >= c_iota
    lower = causal.astype(jnp.bfloat16)
    upper = (r_iota <= c_iota).astype(jnp.bfloat16)
    hi, lo = split(m.spike[...])
    spike_col = mm(lower, hi) + mm(lower, lo)
    hi, lo = split(m.spike_t[...])
    spike_row = mm(hi, upper) + mm(lo, upper)
    for h in range(rec_heads):
        ks = slice(h * REC_KEY, (h + 1) * REC_KEY)
        vs = slice(h * REC_VAL, (h + 1) * REC_VAL)
        q = m.pr[:, ks].astype(jnp.float32)
        lifted = q * jax.nn.sigmoid(q)
        intake = (1.0 - m.low[h : h + 1, :]) * jax.nn.sigmoid(-m.pf[:, ks].astype(jnp.float32))
        hi, lo = split(jnp.log1p(-intake))
        run = mm(lower, hi) + mm(lower, lo)
        s_col = spike_col[:, h : h + 1]
        s_row = spike_row[h : h + 1, :]
        q_up = lifted * jnp.exp(run)
        k_down = (intake * jnp.exp(-run)).astype(jnp.bfloat16)
        decay = jnp.exp(jnp.where(causal, s_col - s_row, 0.0))
        inner = jnp.where(causal, mm(q_up.astype(jnp.bfloat16), k_down, NT) * decay, 0.0)
        v = m.pi[:, vs]
        m.local_out[:, vs] = mm(inner.astype(jnp.bfloat16), v)
        m.qdec[:, ks] = (q_up * jnp.exp(s_col)).astype(jnp.bfloat16)
        total = run[rows - 1 : rows, :] + s_col[rows - 1 : rows, :]
        k_end = (intake * jnp.exp(total - (run + s_col))).astype(jnp.bfloat16)
        state = mm(v, k_end, TN).astype(jnp.bfloat16)
        tail = tail_of(total)
        for i in range(GROUP):
            m.s_own[i, 0:span, ks] = state[i * span : (i + 1) * span]
            m.s_own[i, span:, ks] = tail

    def s_copy(off):
        return remote(
            m.s_own.at[lax.rem(g + off, GROUP)], m.s_mates.at[g], m.s_send.at[off], m.s_recv.at[off], sp=mate(off)
        )

    def p_copy(plane):
        return remote(m.p_own, m.p_planes.at[z], m.p_send.at[plane], m.p_recv.at[z], sp=plane * GROUP + g)

    def p_arrival(plane):
        return remote(m.p_own, m.p_planes.at[plane], m.p_send.at[plane], m.p_recv.at[plane], sp=behind)

    def i_copy(off):
        return remote(
            m.i_own.at[lax.rem(g + off, GROUP)], m.i_mates.at[g], m.i_send.at[off], m.i_recv.at[off], sp=mate(off)
        )

    start([s_copy(off) for off in range(1, GROUP)])
    m.s_mates[g] = m.s_own[g]

    for name, place in (("q", None), ("g", m.pg)):
        for cut in tiles(name):
            done = project(name, cut)
            if place is not None:
                place[:, cut] = done
            else:
                for h in range(heads):
                    if cut.start <= h * HEAD < cut.stop:
                        m.qh[h] = done[:, h * HEAD - cut.start : (h + 1) * HEAD - cut.start]

    def parts(packed):
        return packed[0:span].astype(jnp.float32), jnp.sum(packed[span:].astype(jnp.float32), axis=0, keepdims=True)

    def append(state, packed):
        added, total = parts(packed)
        return state * jnp.exp(total) + added

    for off in range(1, GROUP):
        s_copy(off).wait_recv()
    state, total = parts(m.s_mates[0])
    for i in range(1, GROUP):
        state = append(state, m.s_mates[i])
        total = total + parts(m.s_mates[i])[1]
    m.p_own[0:span] = state.astype(jnp.bfloat16)
    m.p_own[span:] = tail_of(total)

    @pl.loop(z + 1, planes)
    def _(plane):
        p_copy(plane).start()

    sums = jnp.where(r_iota > c_iota, -1.0, 0.0).astype(jnp.bfloat16)
    before = c_iota < r_iota

    def attend(numbers, first):
        scores, stays = [], []
        for number in numbers:
            for h in range(heads):
                hs = slice(h * HEAD, (h + 1) * HEAD)
                k = jnp.concatenate([m.kv[number, r, hs, :] for r in range(chunks)], axis=1)
                s = mm(m.qh[h], k) * (HEAD**-0.5 * LOG2E) + m.bias[h] * LOG2E
                soft = jnp.maximum(s, jnp.log2(1.0 + jnp.exp2(jnp.minimum(s, 100.0))))
                scores.append(s - soft)
                stays.append(jnp.where(before, soft, 0.0) if first else soft)
        for i, (score, stay) in enumerate(zip(scores, stays)):
            number, h = numbers[i // heads], i % heads
            vs = slice(width + h * HEAD, width + (h + 1) * HEAD)
            v = jnp.concatenate([m.kv[number, r, vs, :] for r in range(chunks)], axis=1)
            later = mm(stay.astype(jnp.bfloat16), sums)
            w = jnp.exp2(score + later)
            if first:
                w = jnp.where(before, w, 0.0)
            o = mm(w.astype(jnp.bfloat16), v, NT)
            every = jnp.broadcast_to((later - stay)[:, 0:1], (rows, HEAD))
            if first:
                m.acc[h] = o
                m.carry[h] = every
            else:
                m.acc[h] += o * jnp.exp2(m.carry[h])
                m.carry[h] += every

    attend([me], True)

    @pl.when(c == 1)
    def _():
        from_sibling(z, y)
        attend([me - 1], False)

    @pl.loop(0, z)
    def _(plane):
        p_arrival(plane).wait_recv()

    state = lax.fori_loop(
        0, z, lambda plane, so_far: append(so_far, m.p_planes[plane]), jnp.zeros((span, wide), jnp.float32)
    )
    for i in range(GROUP):
        m.i_own[i] = state.astype(jnp.bfloat16)
        state = append(state, m.s_mates[i])
    start([i_copy(off) for off in range(1, GROUP)])
    m.i_mates[g] = m.i_own[g]

    @pl.when((z == 0) & (y == 0))
    def _():
        event(0, 1)

    early = (z == planes - 1) & (z > 1)

    @pl.loop(2 - y, 2 * z + 2)
    def _(step):
        d, ys = step // 2, 1 - lax.rem(step, 2)
        zs = z - d

        @pl.when((ys == 1) & (d > 0) & ~(early & (zs == 0)))
        def _():
            event(zs, y)

        @pl.when((ys != y) & ~(early & (zs == 0)))
        def _():
            event(zs, 1 - y)

        @pl.when(early & (d == 1) & (ys == 1))
        def _():
            event(0, y)

        @pl.when(early & (d == 2) & (ys == 1))
        def _():
            event(0, 1 - y)

        from_sibling(zs, ys)
        attend([zs * GROUP + ys * 2 + 1, zs * GROUP + ys * 2], False)

    for off in range(1, GROUP):
        i_copy(off).wait_recv()
    for h in range(rec_heads):
        ks = slice(h * REC_KEY, (h + 1) * REC_KEY)
        vs = slice(h * REC_VAL, (h + 1) * REC_VAL)
        entering = jnp.concatenate([m.i_mates[i, :, ks] for i in range(GROUP)], axis=0)
        raw = m.local_out[:, vs] + mm(m.qdec[:, ks], entering, NT)
        gate = m.pg[:, vs].astype(jnp.float32)
        mean = jnp.sum(raw * raw, axis=1, keepdims=True) * (1.0 / REC_VAL)
        done = raw * lax.rsqrt(mean + epsilon) * m.norm[...] * (gate * jax.nn.sigmoid(gate))
        m.rec[t, :, vs] = done.astype(jnp.bfloat16)

    def head_copy(i, shift):
        piece = (m.att, m.rec)[i].at[t]
        return remote(piece, piece, m.head_send.at[i, shift], m.head_recv.at[i, shift], tp=partner(shift))

    start([head_copy(1, shift) for shift in range(1, tp)])
    m.att[t] = jnp.concatenate([m.acc[h] for h in range(heads)], axis=1).astype(jnp.bfloat16)
    start([head_copy(0, shift) for shift in range(1, tp)])
    for one in load_outer:
        one.wait()
    mixed = mm(m.att[t], m.win[t, 0]) + mm(m.rec[t], m.win[t, 1])
    for shift in range(1, tp):
        slot = lax.rem(t + tp - shift, tp)
        outer_copy(shift, outer[0], 0).wait_recv()
        outer_share(shift).start()
        outer_share(shift).wait_recv()
        for i in (1, 0):
            head_copy(i, shift).wait_recv()
        mixed = mixed + mm(m.rec[slot], m.win[slot, 1]) + mm(m.att[slot], m.win[slot, 0])
    m.out[...] = mixed.astype(jnp.bfloat16)

    sent(token_sends)
    sent([s_copy(off) for off in range(1, GROUP)] + [i_copy(off) for off in range(1, GROUP)])
    sent([head_copy(i, shift) for i in (0, 1) for shift in range(1, tp)])
    sent([outer_share(shift) for shift in range(1, tp)] + [outer_copy(shift, outer[0], 0) for shift in range(1, tp)])

    @pl.loop(z + 1, planes)
    def _(plane):
        p_copy(plane).wait_send()

    @pl.loop(0, z + 1)
    def _(zs):
        for r in range(chunks):
            relay(zs, y, r, lambda one: one.wait_send())

            @pl.when((zs < z) | (y == 1) | (z == 0))
            def _():
                relay(zs, 1 - y, r, lambda one: one.wait_send())


def shards(sp, tp, *arrays):
    (tokens, gain, wq, wk, wv, bias, wr, wf, wi, wg, low, spike, norm, attention_out, recurrence_out) = arrays
    rows, features = tokens.shape
    width, wide, narrow = wq.shape[1], wr.shape[1], wi.shape[1]
    heads = width // HEAD
    columns = attention_out.shape[1] // tp
    chunk = min(LANES, rows)
    chunks = rows // chunk
    planes = sp // GROUP
    bf16, f32, dma = jnp.bfloat16, jnp.float32, pltpu.SemaphoreType.DMA
    inputs = dict(
        tokens=tokens,
        gain=gain.reshape(1, -1),
        hbm_k=wk,
        hbm_v=wv,
        hbm_q=wq,
        hbm_r=wr,
        hbm_f=wf,
        hbm_i=wi,
        hbm_g=wg,
        bias=bias,
        low=low,
        spike=spike,
        spike_t=spike.T,
        norm=norm.reshape(1, -1),
        hbm_attention_out=attention_out,
        hbm_recurrence_out=recurrence_out,
    )
    in_hbm = [name == "tokens" or name.startswith("hbm") for name in inputs]
    specs = [SMEM if name == "bias" else ANY if hbm else VMEM for name, hbm in zip(inputs, in_hbm)]
    scratch = dict(tok=pltpu.VMEM((tp, rows, features), bf16))
    sizes = dict(k=width, v=width, q=width, r=wide, f=wide, i=narrow, g=narrow)
    for name, size in sizes.items():
        scratch["w" + name] = pltpu.VMEM((features * tp, size), bf16)
        scratch["a" + name] = pltpu.VMEM((rows, size), f32)
        if name in "rfig":
            scratch["p" + name] = pltpu.VMEM((rows, size), bf16)
    scratch.update(
        own_scaled=pltpu.VMEM((rows, features), bf16),
        far_scaled=pltpu.VMEM((rows, features), bf16),
        square=pltpu.VMEM((rows, LANES), f32),
        kv=pltpu.VMEM((sp, chunks, 2 * width, chunk), bf16),
        qh=pltpu.VMEM((heads, rows, HEAD), bf16),
        acc=pltpu.VMEM((heads, rows, HEAD), f32),
        carry=pltpu.VMEM((heads, rows, HEAD), f32),
        local_out=pltpu.VMEM((rows, narrow), f32),
        qdec=pltpu.VMEM((rows, wide), bf16),
        s_own=pltpu.VMEM((GROUP, REC_VAL // GROUP + TAIL, wide), bf16),
        s_mates=pltpu.VMEM((GROUP, REC_VAL // GROUP + TAIL, wide), bf16),
        p_own=pltpu.VMEM((REC_VAL // GROUP + TAIL, wide), bf16),
        p_planes=pltpu.VMEM((planes, REC_VAL // GROUP + TAIL, wide), bf16),
        i_own=pltpu.VMEM((GROUP, REC_VAL // GROUP, wide), bf16),
        i_mates=pltpu.VMEM((GROUP, REC_VAL // GROUP, wide), bf16),
        win=pltpu.VMEM((tp, 2, width, columns), bf16),
        att=pltpu.VMEM((tp, rows, width), bf16),
        rec=pltpu.VMEM((tp, rows, narrow), bf16),
        load_sem=dma((10,)),
        tok_send=dma((tp, chunks)),
        tok_recv=dma((tp, chunks)),
        kv_send=dma((4, sp, chunks)),
        kv_recv=dma((sp, chunks)),
        s_send=dma((GROUP,)),
        s_recv=dma((GROUP,)),
        p_send=dma((planes,)),
        p_recv=dma((planes,)),
        i_send=dma((GROUP,)),
        i_recv=dma((GROUP,)),
        outer_send=dma((tp, 2)),
        outer_recv=dma((tp, 2)),
        head_send=dma((2, tp)),
        head_recv=dma((2, tp)),
    )
    return pl.pallas_call(
        functools.partial(layer_kernel, sp, tp, list(inputs) + ["out"] + list(scratch)),
        out_shape=jax.ShapeDtypeStruct((rows, columns), bf16),
        in_specs=specs,
        out_specs=VMEM,
        scratch_shapes=list(scratch.values()),
        compiler_params=pltpu.CompilerParams(
            collective_id=0, has_side_effects=True, vmem_limit_bytes=60 * 1024 * 1024
        ),
        name="layer",
    )(*inputs.values())


def solution(mesh):
    placed = (
        P("sp", "tp"),
        P(),
        P(None, "tp"),
        P(None, "tp"),
        P(None, "tp"),
        P("tp"),
        P(None, "tp"),
        P(None, "tp"),
        P(None, "tp"),
        P(None, "tp"),
        P("tp", None),
        P("sp", "tp"),
        P(),
        P("tp", None),
        P("tp", None),
    )
    return jax.shard_map(
        functools.partial(shards, mesh.shape["sp"], mesh.shape["tp"]),
        mesh=mesh,
        in_specs=placed,
        out_specs=P("sp", "tp"),
        check_vma=False,
    )
```

time: 103 us -> 72.8 us (0.71)
  the two profiles are of different devices: /device:TPU:29 before, /device:TPU:18 now
where the time goes in v1:
time: 72.8 us; the launch traced here: 71.9 us
  Pallas kernels  68.6 us (94%)
  local copies, waits for them, and re-layouts  3.35 us (5%)
    pallas_call x1, Pallas kernels, shards(): pl.pallas_call(functools.partial(layer_kernel, sp, tp, list(inputs) + ['o...  68.6 us
    unnamed x2, local copies, waits for them, and re-layouts  3.35 us

profile of v1, /device:TPU:18, one launch (start us, length us, event | category | flops | bytes accessed | tf_op | source)
XLA Modules:
  0.0 71.9 jit_solution(9977751756055616748)
XLA Ops:
  0.0 1.5 %copy.16.refs_11_ = f32[256,4]{1,0:T(8,128)} copy(f32[256,4]{0,1:T(4,128)} %param.26) | data formatting | bytes 8192 | tf_op args[11]
  1.5 68.6 %layer.1 = bf16[256,1024]{1,0:T(8,128)(2,1)} custom-call(bf16[256,1024]{1,0:T(8,128)(2,1)} %refs_0_.1, f32[1,2048]{1,0:T(1,128)} %bitcast.4, bf16[2048,256]{1,0:T(8,128)(2,1)} %refs_2_.1, bf16[2048,256]{1,0:T(8,128)(2,1)} %refs_3_.1, bf16[2048,256]{1,0:T(8,128)(2,1)} %refs_4_.1, bf16[2048,512]{1,0:T(8,128)(2,1)} %refs_5_.1, bf16[2048,512]{1,0:T(8,128)(2,1)} %refs_6_.1, ...), custom_call_target="tpu_custom_call" | custom-call | tf_op jit(solution)/shard_map/layer/pallas_call | solution.py:514
  70.1 1.9 %copy.18 = bf16[256,1024]{1,0:T(8,128)(2,1)} copy(bf16[256,1024]{1,0:T(8,128)(2,1)} %layer.1) | data formatting | bytes 1048576

commit v2 on v1

--- a/solution.py
+++ b/solution.py
@@ -73,7 +73,7 @@
     heads, rec_heads = width // HEAD, narrow // REC_VAL
     chunks, chunk = m.kv.shape[1], m.kv.shape[3]
     planes = sp // GROUP
-    half = planes // 2
+    lend = planes > 2
     columns = m.out.shape[1]
     span = REC_VAL // GROUP
     me, t = lax.axis_index("sp"), lax.axis_index("tp")
@@ -81,7 +81,8 @@
     g = lax.rem(me, GROUP)
     sibling, across = me + 1 - 2 * c, z * GROUP + (1 - y) * 2 + c
     ahead = lax.rem(z + 1, planes) * GROUP + g
-    behind = lax.rem(z + planes - 1, planes) * GROUP + g
+    bottom, top = g, (planes - 1) * GROUP + g
+    lends, borrows = lend & (z == 0), lend & (z == planes - 1)
 
     def mate(off):
         return z * GROUP + lax.rem(g + off, GROUP)
@@ -150,33 +151,37 @@
 
     def relay(zs, ys, r, act):
         number = zs * GROUP + ys * 2 + c
-        column, first = ys == y, zs == 0
-        here = zs == z
-
-        @pl.when((first & (z + 1 < half)) | (~first & column & (z < planes - 1)))
+        column, here = ys == y, zs == z
+        last = jnp.where(zs == 0, planes - 1 - lend, planes - 1)
+
+        @pl.when(column & (z < last))
         def _():
             act(kv_copy(number, r, 0, ahead))
 
-        @pl.when(column & ((here & ((y == 0) | (z == 0))) | (~here & ~first)))
+        @pl.when(column & (~here | (y == 0) | lends))
         def _():
             act(kv_copy(number, r, 1, across))
 
-        @pl.when(first & ((z == 0) | (z > half)))
-        def _():
-            act(kv_copy(number, r, 2, behind))
-
-        @pl.when(~here | (column & (c == 0)) | (~column & (y == 1)))
-        def _():
-            act(kv_copy(number, r, 3, sibling))
-
-    def event(zs, ys):
-        for r in range(chunks):
+        @pl.when(~here | (column & (c == 0)) | (~column & (y == 1)) | lends)
+        def _():
+            act(kv_copy(number, r, 2, sibling))
+
+    def event(cond, zs, ys, r):
+        @pl.when(cond & ~(borrows & (zs == 0)))
+        def _():
             kv_copy(zs * GROUP + ys * 2 + c, r, 0, ahead).wait_recv()
             relay(zs, ys, r, lambda one: one.start())
 
+    def facing(w):
+        return (w <= z + 1) & ((w > 1) | (y == 1) | lends)
+
+    def wave_events(w, r):
+        event(w <= z, z - w, y, r)
+        event(facing(w), z - w + 1, 1 - y, r)
+
     def from_sibling(zs, ys):
         for r in range(chunks):
-            kv_copy(zs * GROUP + ys * 2 + 1 - c, r, 3, sibling).wait_recv()
+            kv_copy(zs * GROUP + ys * 2 + 1 - c, r, 2, sibling).wait_recv()
 
     for shift in range(1, tp):
         slot = lax.rem(t + tp - shift, tp)
@@ -199,6 +204,7 @@
                 for cut in tiles(name):
                     getattr(m, "a" + name)[:, cut] += mm(m.far_scaled[...], weight_rows(name, slot, cut))
     slot = lax.rem(t + 1, tp)
+    wave_events(1, 0)
 
     def outer_copy(shift, array, other):
         from_columns = array.at[:, pl.ds(pl.multiple_of(partner(shift) * columns, columns), columns)]
@@ -222,17 +228,28 @@
         whole = getattr(m, "a" + name)[:, cut] + mm(m.far_scaled[...], weight_rows(name, slot, cut))
         return (whole * inverse).astype(jnp.bfloat16)
 
-    for name in "rfi":
+    def query_copy():
+        return remote(m.pq, m.far_q, m.lend_send.at[0], m.lend_recv.at[0], sp=bottom)
+
+    def lent_copy():
+        return remote(m.lent, m.lent_back, m.lend_send.at[1], m.lend_recv.at[1], sp=top)
+
+    for name in "qrfig":
         for cut in tiles(name):
             getattr(m, "p" + name)[:, cut] = project(name, cut)
+        if name == "q":
+
+            @pl.when(borrows)
+            def _():
+                query_copy().start()
 
     r_iota, c_iota = iota((rows, rows), 0), iota((rows, rows), 1)
     causal = r_iota >= c_iota
     lower = causal.astype(jnp.bfloat16)
     upper = (r_iota <= c_iota).astype(jnp.bfloat16)
-    hi, lo = split(m.spike[...])
-    spike_col = mm(lower, hi) + mm(lower, lo)
-    hi, lo = split(m.spike_t[...])
+    spikes = m.spike_t[...] if rec_heads > 1 else jnp.broadcast_to(m.spike_t[...], (8, rows))
+    hi, lo = split(spikes)
+    spike_col = mm(lower, hi, NT) + mm(lower, lo, NT)
     spike_row = mm(hi, upper) + mm(lo, upper)
     for h in range(rec_heads):
         ks = slice(h * REC_KEY, (h + 1) * REC_KEY)
@@ -268,7 +285,7 @@
         return remote(m.p_own, m.p_planes.at[z], m.p_send.at[plane], m.p_recv.at[z], sp=plane * GROUP + g)
 
     def p_arrival(plane):
-        return remote(m.p_own, m.p_planes.at[plane], m.p_send.at[plane], m.p_recv.at[plane], sp=behind)
+        return remote(m.p_own, m.p_planes.at[plane], m.p_send.at[plane], m.p_recv.at[plane], sp=bottom)
 
     def i_copy(off):
         return remote(
@@ -278,15 +295,11 @@
     start([s_copy(off) for off in range(1, GROUP)])
     m.s_mates[g] = m.s_own[g]
 
-    for name, place in (("q", None), ("g", m.pg)):
-        for cut in tiles(name):
-            done = project(name, cut)
-            if place is not None:
-                place[:, cut] = done
-            else:
-                for h in range(heads):
-                    if cut.start <= h * HEAD < cut.stop:
-                        m.qh[h] = done[:, h * HEAD - cut.start : (h + 1) * HEAD - cut.start]
+    def take_queries(queries):
+        for h in range(heads):
+            m.qh[h] = queries[:, h * HEAD : (h + 1) * HEAD]
+
+    take_queries(m.pq)
 
     def parts(packed):
         return packed[0:span].astype(jnp.float32), jnp.sum(packed[span:].astype(jnp.float32), axis=0, keepdims=True)
@@ -295,23 +308,10 @@
         added, total = parts(packed)
         return state * jnp.exp(total) + added
 
-    for off in range(1, GROUP):
-        s_copy(off).wait_recv()
-    state, total = parts(m.s_mates[0])
-    for i in range(1, GROUP):
-        state = append(state, m.s_mates[i])
-        total = total + parts(m.s_mates[i])[1]
-    m.p_own[0:span] = state.astype(jnp.bfloat16)
-    m.p_own[span:] = tail_of(total)
-
-    @pl.loop(z + 1, planes)
-    def _(plane):
-        p_copy(plane).start()
-
     sums = jnp.where(r_iota > c_iota, -1.0, 0.0).astype(jnp.bfloat16)
     before = c_iota < r_iota
 
-    def attend(numbers, first):
+    def attend(numbers, place, first=False, after=False):
         scores, stays = [], []
         for number in numbers:
             for h in range(heads):
@@ -321,6 +321,7 @@
                 soft = jnp.maximum(s, jnp.log2(1.0 + jnp.exp2(jnp.minimum(s, 100.0))))
                 scores.append(s - soft)
                 stays.append(jnp.where(before, soft, 0.0) if first else soft)
+        done = {}
         for i, (score, stay) in enumerate(zip(scores, stays)):
             number, h = numbers[i // heads], i % heads
             vs = slice(width + h * HEAD, width + (h + 1) * HEAD)
@@ -331,89 +332,151 @@
                 w = jnp.where(before, w, 0.0)
             o = mm(w.astype(jnp.bfloat16), v, NT)
             every = jnp.broadcast_to((later - stay)[:, 0:1], (rows, HEAD))
-            if first:
-                m.acc[h] = o
-                m.carry[h] = every
-            else:
-                m.acc[h] += o * jnp.exp2(m.carry[h])
-                m.carry[h] += every
-
-    attend([me], True)
+            if after:
+                done[h] = m.part[place, h], m.carry[place, h]
+            if h in done:
+                o, every = done[h][0] + o * jnp.exp2(done[h][1]), done[h][1] + every
+            done[h] = o, every
+            if number is numbers[-1]:
+                m.part[place, h], m.carry[place, h] = done[h]
+
+    attend([me], 1 - y, first=True)
 
     @pl.when(c == 1)
     def _():
         from_sibling(z, y)
-        attend([me - 1], False)
-
-    @pl.loop(0, z)
-    def _(plane):
-        p_arrival(plane).wait_recv()
-
-    state = lax.fori_loop(
-        0, z, lambda plane, so_far: append(so_far, m.p_planes[plane]), jnp.zeros((span, wide), jnp.float32)
-    )
-    for i in range(GROUP):
-        m.i_own[i] = state.astype(jnp.bfloat16)
-        state = append(state, m.s_mates[i])
-    start([i_copy(off) for off in range(1, GROUP)])
-    m.i_mates[g] = m.i_own[g]
-
-    @pl.when((z == 0) & (y == 0))
-    def _():
-        event(0, 1)
-
-    early = (z == planes - 1) & (z > 1)
-
-    @pl.loop(2 - y, 2 * z + 2)
-    def _(step):
-        d, ys = step // 2, 1 - lax.rem(step, 2)
-        zs = z - d
-
-        @pl.when((ys == 1) & (d > 0) & ~(early & (zs == 0)))
-        def _():
-            event(zs, y)
-
-        @pl.when((ys != y) & ~(early & (zs == 0)))
-        def _():
-            event(zs, 1 - y)
-
-        @pl.when(early & (d == 1) & (ys == 1))
-        def _():
-            event(0, y)
-
-        @pl.when(early & (d == 2) & (ys == 1))
-        def _():
-            event(0, 1 - y)
-
-        from_sibling(zs, ys)
-        attend([zs * GROUP + ys * 2 + 1, zs * GROUP + ys * 2], False)
-
-    for off in range(1, GROUP):
-        i_copy(off).wait_recv()
-    for h in range(rec_heads):
-        ks = slice(h * REC_KEY, (h + 1) * REC_KEY)
-        vs = slice(h * REC_VAL, (h + 1) * REC_VAL)
-        entering = jnp.concatenate([m.i_mates[i, :, ks] for i in range(GROUP)], axis=0)
-        raw = m.local_out[:, vs] + mm(m.qdec[:, ks], entering, NT)
-        gate = m.pg[:, vs].astype(jnp.float32)
-        mean = jnp.sum(raw * raw, axis=1, keepdims=True) * (1.0 / REC_VAL)
-        done = raw * lax.rsqrt(mean + epsilon) * m.norm[...] * (gate * jax.nn.sigmoid(gate))
-        m.rec[t, :, vs] = done.astype(jnp.bfloat16)
+        attend([me - 1], 1 - y, after=True)
+
+    def gather_states():
+        for off in range(1, GROUP):
+            s_copy(off).wait_recv()
+        state, total = parts(m.s_mates[0])
+        for i in range(1, GROUP):
+            state = append(state, m.s_mates[i])
+            total = total + parts(m.s_mates[i])[1]
+        m.p_own[0:span] = state.astype(jnp.bfloat16)
+        m.p_own[span:] = tail_of(total)
+
+        @pl.loop(z + 1, planes)
+        def _(plane):
+            p_copy(plane).start()
+
+    def enter_states():
+        @pl.loop(0, z)
+        def _(plane):
+            p_arrival(plane).wait_recv()
+
+        state = lax.fori_loop(
+            0, z, lambda plane, so_far: append(so_far, m.p_planes[plane]), jnp.zeros((span, wide), jnp.float32)
+        )
+        for i in range(GROUP):
+            m.i_own[i] = state.astype(jnp.bfloat16)
+            state = append(state, m.s_mates[i])
+        start([i_copy(off) for off in range(1, GROUP)])
+        m.i_mates[g] = m.i_own[g]
 
     def head_copy(i, shift):
         piece = (m.att, m.rec)[i].at[t]
         return remote(piece, piece, m.head_send.at[i, shift], m.head_recv.at[i, shift], tp=partner(shift))
 
-    start([head_copy(1, shift) for shift in range(1, tp)])
-    m.att[t] = jnp.concatenate([m.acc[h] for h in range(heads)], axis=1).astype(jnp.bfloat16)
+    def finish_states():
+        for off in range(1, GROUP):
+            i_copy(off).wait_recv()
+        for h in range(rec_heads):
+            ks = slice(h * REC_KEY, (h + 1) * REC_KEY)
+            vs = slice(h * REC_VAL, (h + 1) * REC_VAL)
+            entering = jnp.concatenate([m.i_mates[i, :, ks] for i in range(GROUP)], axis=0)
+            raw = m.local_out[:, vs] + mm(m.qdec[:, ks], entering, NT)
+            gate = m.pg[:, vs].astype(jnp.float32)
+            mean = jnp.sum(raw * raw, axis=1, keepdims=True) * (1.0 / REC_VAL)
+            done = raw * lax.rsqrt(mean + epsilon) * m.norm[...] * (gate * jax.nn.sigmoid(gate))
+            m.rec[t, :, vs] = done.astype(jnp.bfloat16)
+        start([head_copy(1, shift) for shift in range(1, tp)])
+
+    @pl.loop(1, z + 2)
+    def _(w):
+        for r in range(1, chunks):
+            wave_events(w, r)
+
+        @pl.when(w == 3)
+        def _():
+            finish_states()
+
+        @pl.loop(0, 2)
+        def _(i):
+            zs, ys = z - w + 1 - i, jnp.where(i == 0, 1 - y, y)
+
+            @pl.when((zs >= 0) & ((i == 1) | (w > 1) | (y == 1)) & ~(borrows & (zs == 0)))
+            def _():
+                from_sibling(zs, ys)
+                attend([zs * GROUP + ys * 2 + 1, zs * GROUP + ys * 2], 2 * (z - zs) + 1 - ys)
+
+            @pl.when((w == 2) & (i == 0))
+            def _():
+                enter_states()
+
+        wave_events(w + 1, 0)
+
+        @pl.when(w == 1)
+        def _():
+            gather_states()
+
+    @pl.when(z == 0)
+    def _():
+        enter_states()
+
+    if lend:
+
+        @pl.when(z == 0)
+        def _():
+            query_copy().wait_recv()
+            take_queries(m.far_q)
+
+            @pl.when(c == 0)
+            def _():
+                from_sibling(0, y)
+
+            @pl.when(y == 0)
+            def _():
+                from_sibling(0, 1)
+
+            @pl.loop(0, 2)
+            def _(i):
+                attend([3 - 2 * i, 2 - 2 * i], 2 + i)
+
+            for h in range(heads):
+                whole = m.part[2, h] + m.part[3, h] * jnp.exp2(m.carry[2, h])
+                m.lent[:, h * HEAD : (h + 1) * HEAD] = whole.astype(jnp.bfloat16)
+            lent_copy().start()
+
+    @pl.when(z < 2)
+    def _():
+        finish_states()
+
+    for shift in range(1, tp):
+        outer_copy(shift, outer[0], 0).wait_recv()
+        outer_share(shift).start()
+
+    @pl.loop(2 - y, 2 * z + 2 - 2 * borrows.astype(jnp.int32))
+    def _(place):
+        for h in range(heads):
+            m.part[1 - y, h] += m.part[place, h] * jnp.exp2(m.carry[1 - y, h])
+            m.carry[1 - y, h] += m.carry[place, h]
+
+    @pl.when(borrows)
+    def _():
+        lent_copy().wait_recv()
+        for h in range(heads):
+            lent = m.lent_back[:, h * HEAD : (h + 1) * HEAD].astype(jnp.float32)
+            m.part[1 - y, h] += lent * jnp.exp2(m.carry[1 - y, h])
+
+    m.att[t] = jnp.concatenate([m.part[1 - y, h] for h in range(heads)], axis=1).astype(jnp.bfloat16)
     start([head_copy(0, shift) for shift in range(1, tp)])
     for one in load_outer:
         one.wait()
     mixed = mm(m.att[t], m.win[t, 0]) + mm(m.rec[t], m.win[t, 1])
     for shift in range(1, tp):
         slot = lax.rem(t + tp - shift, tp)
-        outer_copy(shift, outer[0], 0).wait_recv()
-        outer_share(shift).start()
         outer_share(shift).wait_recv()
         for i in (1, 0):
             head_copy(i, shift).wait_recv()
@@ -429,14 +492,22 @@
     def _(plane):
         p_copy(plane).wait_send()
 
-    @pl.loop(0, z + 1)
+    @pl.loop(borrows.astype(jnp.int32), z + 1)
     def _(zs):
         for r in range(chunks):
             relay(zs, y, r, lambda one: one.wait_send())
 
-            @pl.when((zs < z) | (y == 1) | (z == 0))
+            @pl.when((zs < z) | (y == 1) | lends)
             def _():
                 relay(zs, 1 - y, r, lambda one: one.wait_send())
+
+    @pl.when(borrows)
+    def _():
+        query_copy().wait_send()
+
+    @pl.when(lends)
+    def _():
+        lent_copy().wait_send()
 
 
 def shards(sp, tp, *arrays):
@@ -461,7 +532,6 @@
         hbm_g=wg,
         bias=bias,
         low=low,
-        spike=spike,
         spike_t=spike.T,
         norm=norm.reshape(1, -1),
         hbm_attention_out=attention_out,
@@ -474,7 +544,7 @@
     for name, size in sizes.items():
         scratch["w" + name] = pltpu.VMEM((features * tp, size), bf16)
         scratch["a" + name] = pltpu.VMEM((rows, size), f32)
-        if name in "rfig":
+        if name in "qrfig":
             scratch["p" + name] = pltpu.VMEM((rows, size), bf16)
     scratch.update(
         own_scaled=pltpu.VMEM((rows, features), bf16),
@@ -482,8 +552,8 @@
         square=pltpu.VMEM((rows, LANES), f32),
         kv=pltpu.VMEM((sp, chunks, 2 * width, chunk), bf16),
         qh=pltpu.VMEM((heads, rows, HEAD), bf16),
-        acc=pltpu.VMEM((heads, rows, HEAD), f32),
-        carry=pltpu.VMEM((heads, rows, HEAD), f32),
+        part=pltpu.VMEM((max(4, 2 * planes), heads, rows, HEAD), f32),
+        carry=pltpu.VMEM((max(4, 2 * planes), heads, rows, HEAD), f32),
         local_out=pltpu.VMEM((rows, narrow), f32),
         qdec=pltpu.VMEM((rows, wide), bf16),
         s_own=pltpu.VMEM((GROUP, REC_VAL // GROUP + TAIL, wide), bf16),
@@ -493,12 +563,17 @@
         i_own=pltpu.VMEM((GROUP, REC_VAL // GROUP, wide), bf16),
         i_mates=pltpu.VMEM((GROUP, REC_VAL // GROUP, wide), bf16),
         win=pltpu.VMEM((tp, 2, width, columns), bf16),
+        far_q=pltpu.VMEM((rows, width), bf16),
+        lent=pltpu.VMEM((rows, width), bf16),
+        lent_back=pltpu.VMEM((rows, width), bf16),
         att=pltpu.VMEM((tp, rows, width), bf16),
         rec=pltpu.VMEM((tp, rows, narrow), bf16),
         load_sem=dma((10,)),
         tok_send=dma((tp, chunks)),
         tok_recv=dma((tp, chunks)),
-        kv_send=dma((4, sp, chunks)),
+        kv_send=dma((3, sp, chunks)),
+        lend_send=dma((2,)),
+        lend_recv=dma((2,)),
         kv_recv=dma((sp, chunks)),
         s_send=dma((GROUP,)),
         s_recv=dma((GROUP,)),

time: 72.8 us -> 47.6 us (0.65)
  Pallas kernels: 68.6 us -> 45.2 us
  local copies, waits for them, and re-layouts: 3.35 us -> 1.87 us
    pallas_call x1, Pallas kernels: 68.6 us -> 45.2 us  [shards(): pl.pallas_call(functools.partial(layer_kernel, sp, tp, list(inputs) + ['o...]
    unnamed x2 -> x1, local copies, waits for them, and re-layouts: 3.35 us -> 1.87 us
where the time goes in v2:
time: 47.6 us; the launch traced here: 47 us
  Pallas kernels  45.2 us (95%)
  local copies, waits for them, and re-layouts  1.87 us (4%)
    pallas_call x1, Pallas kernels, shards(): pl.pallas_call(functools.partial(layer_kernel, sp, tp, list(inputs) + ['o...  45.2 us
    unnamed x1, local copies, waits for them, and re-layouts  1.87 us

profile of v2, /device:TPU:18, one launch (start us, length us, event | category | flops | bytes accessed | tf_op | source)
XLA Modules:
  0.0 47.0 jit_solution(7530821978382993006)
XLA Ops:
  0.0 45.2 %layer.1 = bf16[256,1024]{1,0:T(8,128)(2,1)} custom-call(bf16[256,1024]{1,0:T(8,128)(2,1)} %refs_0_.1, f32[1,2048]{1,0:T(1,128)} %bitcast.3, bf16[2048,256]{1,0:T(8,128)(2,1)} %refs_2_.1, bf16[2048,256]{1,0:T(8,128)(2,1)} %refs_3_.1, bf16[2048,256]{1,0:T(8,128)(2,1)} %refs_4_.1, bf16[2048,512]{1,0:T(8,128)(2,1)} %refs_5_.1, bf16[2048,512]{1,0:T(8,128)(2,1)} %refs_6_.1, ...), custom_call_target="tpu_custom_call" | custom-call | tf_op jit(solution)/shard_map/layer/pallas_call | solution.py:589
  45.2 1.9 %copy.17 = bf16[256,1024]{1,0:T(8,128)(2,1)} copy(bf16[256,1024]{1,0:T(8,128)(2,1)} %layer.1) | data formatting | bytes 1048576

commit v3 on v2

--- a/solution.py
+++ b/solution.py
@@ -15,6 +15,7 @@
 LANES = 128
 GROUP = 4
 TAIL = 16
+CHUNKS = 4
 LOG2E = math.log2(math.e)
 epsilon = 1e-06
 VMEM = pl.BlockSpec(memory_space=pltpu.VMEM)
@@ -71,11 +72,13 @@
     rows, features = m.tok.shape[1:]
     width, wide, narrow = m.wk.shape[1], m.wr.shape[1], m.wi.shape[1]
     heads, rec_heads = width // HEAD, narrow // REC_VAL
-    chunks, chunk = m.kv.shape[1], m.kv.shape[3]
+    chunks, chunk = CHUNKS, rows // CHUNKS
     planes = sp // GROUP
     lend = planes > 2
     columns = m.out.shape[1]
     span = REC_VAL // GROUP
+    together = m.att.shape[3] // HEAD
+    batches = [range(h, h + together) for h in range(0, heads, together)]
     me, t = lax.axis_index("sp"), lax.axis_index("tp")
     c, y, z = lax.rem(me, 2), lax.rem(me // 2, 2), me // GROUP
     g = lax.rem(me, GROUP)
@@ -119,7 +122,7 @@
 
     def token_copy(shift, r, slot):
         part = m.tok.at[slot, pl.ds(r * chunk, chunk)]
-        return remote(part, part, m.tok_send.at[shift, r], m.tok_recv.at[shift, r], tp=partner(shift))
+        return remote(part, part, m.tok_send.at[shift - 1], m.tok_recv.at[shift - 1, r], tp=partner(shift))
 
     token_sends = [token_copy(shift, r, t) for shift in range(1, tp) for r in range(chunks)]
     start(token_sends)
@@ -146,25 +149,33 @@
             getattr(m, "a" + name)[:, cut] = mm(m.own_scaled[...], weight_rows(name, t, cut))
 
     def kv_copy(number, r, way, target):
-        piece = m.kv.at[number, r]
-        return remote(piece, piece, m.kv_send.at[way, number, r], m.kv_recv.at[number, r], sp=target)
+        piece = m.kv.at[number, pl.ds(r * chunk, chunk)]
+        kind = number // 2
+        if way == 2:
+            return remote(piece, piece, m.kv_send.at[2, kind], m.sib_recv.at[kind], sp=target)
+        return remote(piece, piece, m.kv_send.at[way, kind], m.kv_recv.at[kind, r], sp=target)
+
+    def kv_whole(number, way):
+        piece, kind = m.kv.at[number], number // 2
+        return remote(piece, piece, m.kv_send.at[way, kind], m.sib_recv.at[kind], sp=sibling)
 
     def relay(zs, ys, r, act):
+        copy = kv_copy if r is not None else lambda number, r, way, target: kv_whole(number, way)
         number = zs * GROUP + ys * 2 + c
         column, here = ys == y, zs == z
         last = jnp.where(zs == 0, planes - 1 - lend, planes - 1)
 
         @pl.when(column & (z < last))
         def _():
-            act(kv_copy(number, r, 0, ahead))
+            act(copy(number, r, 0, ahead))
 
         @pl.when(column & (~here | (y == 0) | lends))
         def _():
-            act(kv_copy(number, r, 1, across))
+            act(copy(number, r, 1, across))
 
         @pl.when(~here | (column & (c == 0)) | (~column & (y == 1)) | lends)
         def _():
-            act(kv_copy(number, r, 2, sibling))
+            act(copy(number, r, 2, sibling))
 
     def event(cond, zs, ys, r):
         @pl.when(cond & ~(borrows & (zs == 0)))
@@ -180,8 +191,66 @@
         event(facing(w), z - w + 1, 1 - y, r)
 
     def from_sibling(zs, ys):
-        for r in range(chunks):
-            kv_copy(zs * GROUP + ys * 2 + 1 - c, r, 2, sibling).wait_recv()
+        kv_whole(zs * GROUP + ys * 2 + 1 - c, 2).wait_recv()
+
+    part_rows = rows // 2
+    r_iota, c_iota = iota((part_rows, part_rows), 0), iota((part_rows, part_rows), 1)
+    causal = r_iota >= c_iota
+    lower = causal.astype(jnp.bfloat16)
+    upper = (r_iota <= c_iota).astype(jnp.bfloat16)
+
+    def project(name, part):
+        inverse = lax.rsqrt(m.square[part, 0:1] * (1.0 / (features * tp)) + epsilon)
+        for cut in tiles(name):
+            whole = getattr(m, "a" + name)[part, cut] + mm(
+                m.far_scaled[part], weight_rows(name, lax.rem(t + 1, tp), cut)
+            )
+            getattr(m, "p" + name)[part, cut] = (whole * inverse).astype(jnp.bfloat16)
+
+    def recur(which):
+        part = slice(which * part_rows, (which + 1) * part_rows)
+        spikes = m.spike_t[:, part]
+        if rec_heads == 1:
+            spikes = jnp.broadcast_to(spikes, (8, part_rows))
+        hi, lo = split(spikes)
+        spike_col = mm(lower, hi, NT) + mm(lower, lo, NT)
+        spike_row = mm(hi, upper) + mm(lo, upper)
+        for h in range(rec_heads):
+            ks = slice(h * REC_KEY, (h + 1) * REC_KEY)
+            vs = slice(h * REC_VAL, (h + 1) * REC_VAL)
+            q = m.pr[part, ks].astype(jnp.float32)
+            lifted = q * jax.nn.sigmoid(q)
+            intake = (1.0 - m.low[h : h + 1, :]) * jax.nn.sigmoid(-m.pf[part, ks].astype(jnp.float32))
+            hi, lo = split(jnp.log1p(-intake))
+            run = mm(lower, hi) + mm(lower, lo)
+            s_col = spike_col[:, h : h + 1]
+            s_row = spike_row[h : h + 1, :]
+            q_up = lifted * jnp.exp(run)
+            k_down = (intake * jnp.exp(-run)).astype(jnp.bfloat16)
+            decay = jnp.exp(jnp.where(causal, s_col - s_row, 0.0))
+            inner = jnp.where(causal, mm(q_up.astype(jnp.bfloat16), k_down, NT) * decay, 0.0)
+            v = m.pi[part, vs]
+            output = mm(inner.astype(jnp.bfloat16), v)
+            decayed = q_up * jnp.exp(s_col)
+            total = run[part_rows - 1 : part_rows, :] + s_col[part_rows - 1 : part_rows, :]
+            k_end = (intake * jnp.exp(total - (run + s_col))).astype(jnp.bfloat16)
+            state = mm(v, k_end, TN)
+            if which == 0:
+                m.local_out[part, vs] = output
+                m.qdec[part, ks] = decayed.astype(jnp.bfloat16)
+                m.half_state[:, ks] = state
+                m.half_total[:, ks] = total
+                continue
+            earlier = m.half_state[:, ks]
+            m.local_out[part, vs] = output + mm(decayed.astype(jnp.bfloat16), earlier.astype(jnp.bfloat16), NT)
+            m.qdec[part, ks] = (decayed * jnp.exp(m.half_total[:, ks])).astype(jnp.bfloat16)
+            state = (earlier * jnp.exp(total) + state).astype(jnp.bfloat16)
+            tail = tail_of(total + m.half_total[:, ks])
+            for i in range(GROUP):
+                m.s_own[i, 0:span, ks] = state[i * span : (i + 1) * span]
+                m.s_own[i, span:, ks] = tail
+
+    first_rows, last_rows = slice(0, part_rows), slice(part_rows, rows)
 
     for shift in range(1, tp):
         slot = lax.rem(t + tp - shift, tp)
@@ -197,19 +266,23 @@
                     whole = getattr(m, "a" + name)[part, :] + mm(
                         m.far_scaled[part], weight_rows(name, slot, slice(0, width))
                     )
-                    m.kv[me, r, i * width : (i + 1) * width, :] = (whole * inverse).T.astype(jnp.bfloat16)
+                    m.kv[me, part, i * width : (i + 1) * width] = (whole * inverse).astype(jnp.bfloat16)
                 relay(z, y, r, lambda one: one.start())
+                if 0 < r < chunks - 1:
+                    wave_events(1, r - 1)
+                if r == chunks // 2 - 1:
+                    for name in "qrfi":
+                        project(name, first_rows)
+                    recur(0)
         if shift < tp - 1:
             for name in order:
                 for cut in tiles(name):
                     getattr(m, "a" + name)[:, cut] += mm(m.far_scaled[...], weight_rows(name, slot, cut))
     slot = lax.rem(t + 1, tp)
-    wave_events(1, 0)
-
     def outer_copy(shift, array, other):
         from_columns = array.at[:, pl.ds(pl.multiple_of(partner(shift) * columns, columns), columns)]
         return remote(
-            from_columns, m.win.at[t, other], m.outer_send.at[shift, 0], m.outer_recv.at[shift, 0], tp=partner(shift)
+            from_columns, m.win.at[t, other], m.outer_send.at[shift - 1, 0], m.outer_recv.at[shift - 1, 0], tp=partner(shift)
         )
 
     for which, array in enumerate(outer):
@@ -220,13 +293,7 @@
 
     def outer_share(shift):
         piece = m.win.at[lax.rem(t + tp - shift, tp), c]
-        return remote(piece, piece, m.outer_send.at[shift, 1], m.outer_recv.at[shift, 1], sp=sibling)
-
-    inverse = lax.rsqrt(m.square[:, 0:1] * (1.0 / (features * tp)) + epsilon)
-
-    def project(name, cut):
-        whole = getattr(m, "a" + name)[:, cut] + mm(m.far_scaled[...], weight_rows(name, slot, cut))
-        return (whole * inverse).astype(jnp.bfloat16)
+        return remote(piece, piece, m.outer_send.at[shift - 1, 1], m.outer_recv.at[shift - 1, 1], sp=sibling)
 
     def query_copy():
         return remote(m.pq, m.far_q, m.lend_send.at[0], m.lend_recv.at[0], sp=bottom)
@@ -234,51 +301,19 @@
     def lent_copy():
         return remote(m.lent, m.lent_back, m.lend_send.at[1], m.lend_recv.at[1], sp=top)
 
-    for name in "qrfig":
-        for cut in tiles(name):
-            getattr(m, "p" + name)[:, cut] = project(name, cut)
-        if name == "q":
-
-            @pl.when(borrows)
-            def _():
-                query_copy().start()
-
-    r_iota, c_iota = iota((rows, rows), 0), iota((rows, rows), 1)
-    causal = r_iota >= c_iota
-    lower = causal.astype(jnp.bfloat16)
-    upper = (r_iota <= c_iota).astype(jnp.bfloat16)
-    spikes = m.spike_t[...] if rec_heads > 1 else jnp.broadcast_to(m.spike_t[...], (8, rows))
-    hi, lo = split(spikes)
-    spike_col = mm(lower, hi, NT) + mm(lower, lo, NT)
-    spike_row = mm(hi, upper) + mm(lo, upper)
-    for h in range(rec_heads):
-        ks = slice(h * REC_KEY, (h + 1) * REC_KEY)
-        vs = slice(h * REC_VAL, (h + 1) * REC_VAL)
-        q = m.pr[:, ks].astype(jnp.float32)
-        lifted = q * jax.nn.sigmoid(q)
-        intake = (1.0 - m.low[h : h + 1, :]) * jax.nn.sigmoid(-m.pf[:, ks].astype(jnp.float32))
-        hi, lo = split(jnp.log1p(-intake))
-        run = mm(lower, hi) + mm(lower, lo)
-        s_col = spike_col[:, h : h + 1]
-        s_row = spike_row[h : h + 1, :]
-        q_up = lifted * jnp.exp(run)
-        k_down = (intake * jnp.exp(-run)).astype(jnp.bfloat16)
-        decay = jnp.exp(jnp.where(causal, s_col - s_row, 0.0))
-        inner = jnp.where(causal, mm(q_up.astype(jnp.bfloat16), k_down, NT) * decay, 0.0)
-        v = m.pi[:, vs]
-        m.local_out[:, vs] = mm(inner.astype(jnp.bfloat16), v)
-        m.qdec[:, ks] = (q_up * jnp.exp(s_col)).astype(jnp.bfloat16)
-        total = run[rows - 1 : rows, :] + s_col[rows - 1 : rows, :]
-        k_end = (intake * jnp.exp(total - (run + s_col))).astype(jnp.bfloat16)
-        state = mm(v, k_end, TN).astype(jnp.bfloat16)
-        tail = tail_of(total)
-        for i in range(GROUP):
-            m.s_own[i, 0:span, ks] = state[i * span : (i + 1) * span]
-            m.s_own[i, span:, ks] = tail
+    project("q", last_rows)
+
+    @pl.when(borrows)
+    def _():
+        query_copy().start()
+
+    for name in "rfi":
+        project(name, last_rows)
+    recur(1)
 
     def s_copy(off):
         return remote(
-            m.s_own.at[lax.rem(g + off, GROUP)], m.s_mates.at[g], m.s_send.at[off], m.s_recv.at[off], sp=mate(off)
+            m.s_own.at[lax.rem(g + off, GROUP)], m.s_mates.at[g], m.s_send, m.s_recv.at[off - 1], sp=mate(off)
         )
 
     def p_copy(plane):
@@ -289,10 +324,13 @@
 
     def i_copy(off):
         return remote(
-            m.i_own.at[lax.rem(g + off, GROUP)], m.i_mates.at[g], m.i_send.at[off], m.i_recv.at[off], sp=mate(off)
+            m.i_own.at[lax.rem(g + off, GROUP)], m.i_mates.at[g], m.i_send, m.i_recv.at[off - 1], sp=mate(off)
         )
 
     start([s_copy(off) for off in range(1, GROUP)])
+    project("g", slice(0, rows))
+    wave_events(1, chunks - 2)
+    wave_events(2, 0)
     m.s_mates[g] = m.s_own[g]
 
     def take_queries(queries):
@@ -308,29 +346,28 @@
         added, total = parts(packed)
         return state * jnp.exp(total) + added
 
+    r_iota, c_iota = iota((rows, rows), 0), iota((rows, rows), 1)
     sums = jnp.where(r_iota > c_iota, -1.0, 0.0).astype(jnp.bfloat16)
     before = c_iota < r_iota
 
-    def attend(numbers, place, first=False, after=False):
+    def attend(numbers, place, first=False, after=False, some=range(heads)):
         scores, stays = [], []
         for number in numbers:
-            for h in range(heads):
+            for h in some:
                 hs = slice(h * HEAD, (h + 1) * HEAD)
-                k = jnp.concatenate([m.kv[number, r, hs, :] for r in range(chunks)], axis=1)
-                s = mm(m.qh[h], k) * (HEAD**-0.5 * LOG2E) + m.bias[h] * LOG2E
+                s = mm(m.qh[h], m.kv[number, :, hs], NT) * (HEAD**-0.5 * LOG2E) + m.bias[h] * LOG2E
                 soft = jnp.maximum(s, jnp.log2(1.0 + jnp.exp2(jnp.minimum(s, 100.0))))
                 scores.append(s - soft)
                 stays.append(jnp.where(before, soft, 0.0) if first else soft)
         done = {}
         for i, (score, stay) in enumerate(zip(scores, stays)):
-            number, h = numbers[i // heads], i % heads
+            number, h = numbers[i // len(some)], some[i % len(some)]
             vs = slice(width + h * HEAD, width + (h + 1) * HEAD)
-            v = jnp.concatenate([m.kv[number, r, vs, :] for r in range(chunks)], axis=1)
             later = mm(stay.astype(jnp.bfloat16), sums)
             w = jnp.exp2(score + later)
             if first:
                 w = jnp.where(before, w, 0.0)
-            o = mm(w.astype(jnp.bfloat16), v, NT)
+            o = mm(w.astype(jnp.bfloat16), m.kv[number, :, vs])
             every = jnp.broadcast_to((later - stay)[:, 0:1], (rows, HEAD))
             if after:
                 done[h] = m.part[place, h], m.carry[place, h]
@@ -341,11 +378,25 @@
                 m.part[place, h], m.carry[place, h] = done[h]
 
     attend([me], 1 - y, first=True)
+    wave_events(1, chunks - 1)
+    wave_events(2, 1)
 
     @pl.when(c == 1)
     def _():
         from_sibling(z, y)
         attend([me - 1], 1 - y, after=True)
+
+    def combine(place, some=range(heads)):
+        for h in some:
+            m.part[1 - y, h] += m.part[place, h] * jnp.exp2(m.carry[1 - y, h])
+            m.carry[1 - y, h] += m.carry[place, h]
+
+    def combine_wave(w):
+        for place in (2 * w - 2, 2 * w - 1):
+
+            @pl.when(place > 1 - y)
+            def _():
+                combine(place)
 
     def gather_states():
         for off in range(1, GROUP):
@@ -376,8 +427,8 @@
         m.i_mates[g] = m.i_own[g]
 
     def head_copy(i, shift):
-        piece = (m.att, m.rec)[i].at[t]
-        return remote(piece, piece, m.head_send.at[i, shift], m.head_recv.at[i, shift], tp=partner(shift))
+        piece = m.rec.at[t] if i == len(batches) else m.att.at[t, i]
+        return remote(piece, piece, m.head_send.at[i, shift - 1], m.head_recv.at[i, shift - 1], tp=partner(shift))
 
     def finish_states():
         for off in range(1, GROUP):
@@ -391,12 +442,16 @@
             mean = jnp.sum(raw * raw, axis=1, keepdims=True) * (1.0 / REC_VAL)
             done = raw * lax.rsqrt(mean + epsilon) * m.norm[...] * (gate * jax.nn.sigmoid(gate))
             m.rec[t, :, vs] = done.astype(jnp.bfloat16)
-        start([head_copy(1, shift) for shift in range(1, tp)])
-
-    @pl.loop(1, z + 2)
+        start([head_copy(len(batches), shift) for shift in range(1, tp)])
+
+    waves = z + 1 - borrows.astype(jnp.int32)
+
+    @pl.loop(1, waves + 1)
     def _(w):
-        for r in range(1, chunks):
-            wave_events(w, r)
+        @pl.when(w > 1)
+        def _():
+            combine_wave(w - 1)
+            wave_events(w, chunks - 1)
 
         @pl.when(w == 3)
         def _():
@@ -406,17 +461,25 @@
         def _(i):
             zs, ys = z - w + 1 - i, jnp.where(i == 0, 1 - y, y)
 
-            @pl.when((zs >= 0) & ((i == 1) | (w > 1) | (y == 1)) & ~(borrows & (zs == 0)))
+            @pl.when((i == 1) & (zs >= 0) & ~(borrows & (zs == 0)) | (i == 0) & ((w > 1) | (y == 1)) & (w < waves))
             def _():
                 from_sibling(zs, ys)
                 attend([zs * GROUP + ys * 2 + 1, zs * GROUP + ys * 2], 2 * (z - zs) + 1 - ys)
 
+            @pl.when((w == 1) & (i == 0))
+            def _():
+                for r in range(2, chunks - 1):
+                    wave_events(2, r)
+
+            @pl.when((w > 1) & (i == 0))
+            def _():
+                for r in range(chunks - 1):
+                    wave_events(w + 1, r)
+
             @pl.when((w == 2) & (i == 0))
             def _():
                 enter_states()
 
-        wave_events(w + 1, 0)
-
         @pl.when(w == 1)
         def _():
             gather_states()
@@ -436,9 +499,7 @@
             def _():
                 from_sibling(0, y)
 
-            @pl.when(y == 0)
-            def _():
-                from_sibling(0, 1)
+            from_sibling(0, 1 - y)
 
             @pl.loop(0, 2)
             def _(i):
@@ -448,6 +509,7 @@
                 whole = m.part[2, h] + m.part[3, h] * jnp.exp2(m.carry[2, h])
                 m.lent[:, h * HEAD : (h + 1) * HEAD] = whole.astype(jnp.bfloat16)
             lent_copy().start()
+            take_queries(m.pq)
 
     @pl.when(z < 2)
     def _():
@@ -456,36 +518,69 @@
     for shift in range(1, tp):
         outer_copy(shift, outer[0], 0).wait_recv()
         outer_share(shift).start()
-
-    @pl.loop(2 - y, 2 * z + 2 - 2 * borrows.astype(jnp.int32))
-    def _(place):
-        for h in range(heads):
-            m.part[1 - y, h] += m.part[place, h] * jnp.exp2(m.carry[1 - y, h])
-            m.carry[1 - y, h] += m.carry[place, h]
+    for one in load_outer:
+        one.wait()
+
+    end, last = waves - 1, z - waves + 1
+    facing_end = (waves > 1) | (y == 1)
+
+    @pl.when(facing_end & ~lends)
+    def _():
+        from_sibling(last, 1 - y)
 
     @pl.when(borrows)
     def _():
         lent_copy().wait_recv()
-        for h in range(heads):
-            lent = m.lent_back[:, h * HEAD : (h + 1) * HEAD].astype(jnp.float32)
-            m.part[1 - y, h] += lent * jnp.exp2(m.carry[1 - y, h])
-
-    m.att[t] = jnp.concatenate([m.part[1 - y, h] for h in range(heads)], axis=1).astype(jnp.bfloat16)
-    start([head_copy(0, shift) for shift in range(1, tp)])
-    for one in load_outer:
-        one.wait()
-    mixed = mm(m.att[t], m.win[t, 0]) + mm(m.rec[t], m.win[t, 1])
+
+    for j, some in enumerate(batches):
+
+        @pl.when(facing_end)
+        def _():
+            attend([last * GROUP + (1 - y) * 2 + 1, last * GROUP + (1 - y) * 2], 2 * end + y, some=some)
+
+        for place in (2 * end, 2 * end + 1):
+
+            @pl.when(place > 1 - y)
+            def _():
+                combine(place, some)
+
+        @pl.when(borrows)
+        def _():
+            for h in some:
+                lent = m.lent_back[:, h * HEAD : (h + 1) * HEAD].astype(jnp.float32)
+                m.part[1 - y, h] += lent * jnp.exp2(m.carry[1 - y, h])
+
+        m.att[t, j] = jnp.concatenate([m.part[1 - y, h] for h in some], axis=1).astype(jnp.bfloat16)
+        start([head_copy(j, shift) for shift in range(1, tp)])
+
+    def attention_rows(slot, j):
+        return m.win[slot, 0, HEAD * batches[j][0] : HEAD * (batches[j][-1] + 1), :]
+
+    mixed = mm(m.rec[t], m.win[t, 1])
+    for j in range(len(batches)):
+        mixed = mixed + mm(m.att[t, j], attention_rows(t, j))
     for shift in range(1, tp):
         slot = lax.rem(t + tp - shift, tp)
         outer_share(shift).wait_recv()
-        for i in (1, 0):
-            head_copy(i, shift).wait_recv()
-        mixed = mixed + mm(m.rec[slot], m.win[slot, 1]) + mm(m.att[slot], m.win[slot, 0])
-    m.out[...] = mixed.astype(jnp.bfloat16)
-
-    sent(token_sends)
-    sent([s_copy(off) for off in range(1, GROUP)] + [i_copy(off) for off in range(1, GROUP)])
-    sent([head_copy(i, shift) for i in (0, 1) for shift in range(1, tp)])
+        head_copy(len(batches), shift).wait_recv()
+        mixed = mixed + mm(m.rec[slot], m.win[slot, 1])
+    m.sum[...] = mixed
+    for shift in range(1, tp):
+        slot = lax.rem(t + tp - shift, tp)
+        for j in range(len(batches)):
+            head_copy(j, shift).wait_recv()
+            mixed = mm(m.att[slot, j], attention_rows(slot, j))
+            if shift == tp - 1 and j == len(batches) - 1:
+                m.out[...] = (m.sum[...] + mixed).astype(jnp.bfloat16)
+            else:
+                m.sum[...] += mixed
+
+    for shift in range(1, tp):
+        remote(m.tok.at[t], m.tok.at[t], m.tok_send.at[shift - 1], m.tok_recv.at[0, 0], tp=partner(shift)).wait_send()
+    several = pl.ds(0, GROUP - 1)
+    remote(m.s_own.at[several], m.s_own.at[several], m.s_send, m.s_recv.at[0], sp=sibling).wait_send()
+    remote(m.i_own.at[several], m.i_own.at[several], m.i_send, m.i_recv.at[0], sp=sibling).wait_send()
+    sent([head_copy(i, shift) for i in range(len(batches) + 1) for shift in range(1, tp)])
     sent([outer_share(shift) for shift in range(1, tp)] + [outer_copy(shift, outer[0], 0) for shift in range(1, tp)])
 
     @pl.loop(z + 1, planes)
@@ -494,12 +589,11 @@
 
     @pl.loop(borrows.astype(jnp.int32), z + 1)
     def _(zs):
-        for r in range(chunks):
-            relay(zs, y, r, lambda one: one.wait_send())
-
-            @pl.when((zs < z) | (y == 1) | lends)
-            def _():
-                relay(zs, 1 - y, r, lambda one: one.wait_send())
+        relay(zs, y, None, lambda one: one.wait_send())
+
+        @pl.when((zs < z) | (y == 1) | lends)
+        def _():
+            relay(zs, 1 - y, None, lambda one: one.wait_send())
 
     @pl.when(borrows)
     def _():
@@ -516,9 +610,9 @@
     width, wide, narrow = wq.shape[1], wr.shape[1], wi.shape[1]
     heads = width // HEAD
     columns = attention_out.shape[1] // tp
-    chunk = min(LANES, rows)
-    chunks = rows // chunk
+    chunks = CHUNKS
     planes = sp // GROUP
+    batch = min(LANES, width)
     bf16, f32, dma = jnp.bfloat16, jnp.float32, pltpu.SemaphoreType.DMA
     inputs = dict(
         tokens=tokens,
@@ -550,11 +644,13 @@
         own_scaled=pltpu.VMEM((rows, features), bf16),
         far_scaled=pltpu.VMEM((rows, features), bf16),
         square=pltpu.VMEM((rows, LANES), f32),
-        kv=pltpu.VMEM((sp, chunks, 2 * width, chunk), bf16),
+        kv=pltpu.VMEM((sp, rows, 2 * width), bf16),
         qh=pltpu.VMEM((heads, rows, HEAD), bf16),
         part=pltpu.VMEM((max(4, 2 * planes), heads, rows, HEAD), f32),
         carry=pltpu.VMEM((max(4, 2 * planes), heads, rows, HEAD), f32),
         local_out=pltpu.VMEM((rows, narrow), f32),
+        half_state=pltpu.VMEM((REC_VAL, wide), f32),
+        half_total=pltpu.VMEM((1, wide), f32),
         qdec=pltpu.VMEM((rows, wide), bf16),
         s_own=pltpu.VMEM((GROUP, REC_VAL // GROUP + TAIL, wide), bf16),
         s_mates=pltpu.VMEM((GROUP, REC_VAL // GROUP + TAIL, wide), bf16),
@@ -566,25 +662,27 @@
         far_q=pltpu.VMEM((rows, width), bf16),
         lent=pltpu.VMEM((rows, width), bf16),
         lent_back=pltpu.VMEM((rows, width), bf16),
-        att=pltpu.VMEM((tp, rows, width), bf16),
+        att=pltpu.VMEM((tp, width // batch, rows, batch), bf16),
+        sum=pltpu.VMEM((rows, columns), f32),
         rec=pltpu.VMEM((tp, rows, narrow), bf16),
         load_sem=dma((10,)),
-        tok_send=dma((tp, chunks)),
-        tok_recv=dma((tp, chunks)),
-        kv_send=dma((3, sp, chunks)),
+        tok_send=dma((max(tp - 1, 1),)),
+        tok_recv=dma((max(tp - 1, 1), chunks)),
+        kv_send=dma((3, sp // 2)),
+        kv_recv=dma((sp // 2, chunks)),
+        sib_recv=dma((sp // 2,)),
         lend_send=dma((2,)),
         lend_recv=dma((2,)),
-        kv_recv=dma((sp, chunks)),
-        s_send=dma((GROUP,)),
-        s_recv=dma((GROUP,)),
+        s_send=dma,
+        s_recv=dma((GROUP - 1,)),
         p_send=dma((planes,)),
         p_recv=dma((planes,)),
-        i_send=dma((GROUP,)),
-        i_recv=dma((GROUP,)),
-        outer_send=dma((tp, 2)),
-        outer_recv=dma((tp, 2)),
-        head_send=dma((2, tp)),
-        head_recv=dma((2, tp)),
+        i_send=dma,
+        i_recv=dma((GROUP - 1,)),
+        outer_send=dma((max(tp - 1, 1), 2)),
+        outer_recv=dma((max(tp - 1, 1), 2)),
+        head_send=dma((width // batch + 1, max(tp - 1, 1))),
+        head_recv=dma((width // batch + 1, max(tp - 1, 1))),
     )
     return pl.pallas_call(
         functools.partial(layer_kernel, sp, tp, list(inputs) + ["out"] + list(scratch)),

time: 47.6 us -> 47.8 us (level)
  no operation moved by 1% of the time
where the time goes in v3:
time: 47.8 us; the launch traced here: 47 us
  Pallas kernels  45.1 us (94%)
  local copies, waits for them, and re-layouts  1.87 us (4%)
    pallas_call x1, Pallas kernels, shards(): pl.pallas_call(functools.partial(layer_kernel, sp, tp, list(inputs) + ['o...  45.1 us
    unnamed x1, local copies, waits for them, and re-layouts  1.87 us

profile of v3, /device:TPU:18, one launch (start us, length us, event | category | flops | bytes accessed | tf_op | source)
XLA Modules:
  0.0 47.0 jit_solution(1245262095184626288)
XLA Ops:
  0.0 45.1 %layer.1 = bf16[256,1024]{1,0:T(8,128)(2,1)} custom-call(bf16[256,1024]{1,0:T(8,128)(2,1)} %refs_0_.1, f32[1,2048]{1,0:T(1,128)} %bitcast.3, bf16[2048,256]{1,0:T(8,128)(2,1)} %refs_2_.1, bf16[2048,256]{1,0:T(8,128)(2,1)} %refs_3_.1, bf16[2048,256]{1,0:T(8,128)(2,1)} %refs_4_.1, bf16[2048,512]{1,0:T(8,128)(2,1)} %refs_5_.1, bf16[2048,512]{1,0:T(8,128)(2,1)} %refs_6_.1, ...), custom_call_target="tpu_custom_call" | custom-call | tf_op jit(solution)/shard_map/layer/pallas_call | solution.py:687
  45.1 1.9 %copy.17 = bf16[256,1024]{1,0:T(8,128)(2,1)} copy(bf16[256,1024]{1,0:T(8,128)(2,1)} %layer.1) | data formatting | bytes 1048576

commit v4 on v3

--- a/solution.py
+++ b/solution.py
@@ -309,6 +309,8 @@
 
     for name in "rfi":
         project(name, last_rows)
+    wave_events(1, chunks - 2)
+    wave_events(2, 0)
     recur(1)
 
     def s_copy(off):
@@ -329,8 +331,8 @@
 
     start([s_copy(off) for off in range(1, GROUP)])
     project("g", slice(0, rows))
-    wave_events(1, chunks - 2)
-    wave_events(2, 0)
+    wave_events(1, chunks - 1)
+    wave_events(2, 1)
     m.s_mates[g] = m.s_own[g]
 
     def take_queries(queries):
@@ -378,8 +380,6 @@
                 m.part[place, h], m.carry[place, h] = done[h]
 
     attend([me], 1 - y, first=True)
-    wave_events(1, chunks - 1)
-    wave_events(2, 1)
 
     @pl.when(c == 1)
     def _():

time: 47.8 us -> 45.7 us (0.956); the launches traced: 47 us -> 45.5 us
  Pallas kernels: 45.1 us -> 43.6 us
    pallas_call x1, Pallas kernels: 45.1 us -> 43.6 us  [shards(): pl.pallas_call(functools.partial(layer_kernel, sp, tp, list(inputs) + ['o...]
where the time goes in v4:
time: 45.7 us; the launch traced here: 45.5 us
  Pallas kernels  43.6 us (95%)
  local copies, waits for them, and re-layouts  1.87 us (4%)
    pallas_call x1, Pallas kernels, shards(): pl.pallas_call(functools.partial(layer_kernel, sp, tp, list(inputs) + ['o...  43.6 us
    unnamed x1, local copies, waits for them, and re-layouts  1.87 us

profile of v4, /device:TPU:18, one launch (start us, length us, event | category | flops | bytes accessed | tf_op | source)
XLA Modules:
  0.0 45.5 jit_solution(4297365572921487711)
XLA Ops:
  0.0 43.6 %layer.1 = bf16[256,1024]{1,0:T(8,128)(2,1)} custom-call(bf16[256,1024]{1,0:T(8,128)(2,1)} %refs_0_.1, f32[1,2048]{1,0:T(1,128)} %bitcast.3, bf16[2048,256]{1,0:T(8,128)(2,1)} %refs_2_.1, bf16[2048,256]{1,0:T(8,128)(2,1)} %refs_3_.1, bf16[2048,256]{1,0:T(8,128)(2,1)} %refs_4_.1, bf16[2048,512]{1,0:T(8,128)(2,1)} %refs_5_.1, bf16[2048,512]{1,0:T(8,128)(2,1)} %refs_6_.1, ...), custom_call_target="tpu_custom_call" | custom-call | tf_op jit(solution)/shard_map/layer/pallas_call | solution.py:687
  43.6 1.9 %copy.17 = bf16[256,1024]{1,0:T(8,128)(2,1)} copy(bf16[256,1024]{1,0:T(8,128)(2,1)} %layer.1) | data formatting | bytes 1048576

commit v5 on v4

--- a/solution.py
+++ b/solution.py
@@ -16,6 +16,7 @@
 GROUP = 4
 TAIL = 16
 CHUNKS = 4
+SPIKES, LOWS = 8, 16
 LOG2E = math.log2(math.e)
 epsilon = 1e-06
 VMEM = pl.BlockSpec(memory_space=pltpu.VMEM)
@@ -129,7 +130,7 @@
 
     def scale(slot, part):
         value = m.tok[slot, part, :].astype(jnp.float32)
-        gains = m.gain[:, pl.ds(pl.multiple_of(slot * features, features), features)]
+        gains = m.small[0:1, pl.ds(pl.multiple_of(slot * features, features), features)]
         return (value * gains).astype(jnp.bfloat16), jnp.sum(value * value, axis=1, keepdims=True)
 
     def weight_rows(name, slot, cut):
@@ -209,7 +210,7 @@
 
     def recur(which):
         part = slice(which * part_rows, (which + 1) * part_rows)
-        spikes = m.spike_t[:, part]
+        spikes = m.small[SPIKES : SPIKES + rec_heads, part]
         if rec_heads == 1:
             spikes = jnp.broadcast_to(spikes, (8, part_rows))
         hi, lo = split(spikes)
@@ -220,7 +221,7 @@
             vs = slice(h * REC_VAL, (h + 1) * REC_VAL)
             q = m.pr[part, ks].astype(jnp.float32)
             lifted = q * jax.nn.sigmoid(q)
-            intake = (1.0 - m.low[h : h + 1, :]) * jax.nn.sigmoid(-m.pf[part, ks].astype(jnp.float32))
+            intake = (1.0 - m.small[LOWS + h : LOWS + h + 1, 0:REC_KEY]) * jax.nn.sigmoid(-m.pf[part, ks].astype(jnp.float32))
             hi, lo = split(jnp.log1p(-intake))
             run = mm(lower, hi) + mm(lower, lo)
             s_col = spike_col[:, h : h + 1]
@@ -440,7 +441,7 @@
             raw = m.local_out[:, vs] + mm(m.qdec[:, ks], entering, NT)
             gate = m.pg[:, vs].astype(jnp.float32)
             mean = jnp.sum(raw * raw, axis=1, keepdims=True) * (1.0 / REC_VAL)
-            done = raw * lax.rsqrt(mean + epsilon) * m.norm[...] * (gate * jax.nn.sigmoid(gate))
+            done = raw * lax.rsqrt(mean + epsilon) * m.small[1:2, 0:REC_VAL] * (gate * jax.nn.sigmoid(gate))
             m.rec[t, :, vs] = done.astype(jnp.bfloat16)
         start([head_copy(len(batches), shift) for shift in range(1, tp)])
 
@@ -614,9 +615,17 @@
     planes = sp // GROUP
     batch = min(LANES, width)
     bf16, f32, dma = jnp.bfloat16, jnp.float32, pltpu.SemaphoreType.DMA
+    wide_row = gain.shape[0]
+
+    def padded(array, to_rows):
+        return jnp.pad(array, ((0, to_rows - array.shape[0]), (0, wide_row - array.shape[1])))
+
+    small = jnp.concatenate(
+        [padded(gain[None], 1), padded(norm[None], 7), padded(spike.T, 8), padded(low, 8)], axis=0
+    )
     inputs = dict(
         tokens=tokens,
-        gain=gain.reshape(1, -1),
+        small=small,
         hbm_k=wk,
         hbm_v=wv,
         hbm_q=wq,
@@ -625,9 +634,6 @@
         hbm_i=wi,
         hbm_g=wg,
         bias=bias,
-        low=low,
-        spike_t=spike.T,
-        norm=norm.reshape(1, -1),
         hbm_attention_out=attention_out,
         hbm_recurrence_out=recurrence_out,
     )
@@ -691,7 +697,7 @@
         out_specs=VMEM,
         scratch_shapes=list(scratch.values()),
         compiler_params=pltpu.CompilerParams(
-            collective_id=0, has_side_effects=True, vmem_limit_bytes=60 * 1024 * 1024
+            collective_id=0, has_side_effects=True, vmem_limit_bytes=53 * 1024 * 1024
         ),
         name="layer",
     )(*inputs.values())

time: 45.7 us -> 45 us (0.985)
  Pallas kernels: 43.6 us -> 42.5 us
  other arithmetic: 0 us -> 0.76 us
    pallas_call x1, Pallas kernels: 43.6 us -> 42.5 us  [shards(): pl.pallas_call(functools.partial(layer_kernel, sp, tp, list(inputs) + ['o...]
    concatenate x0 -> x1, other arithmetic: none -> 0.76 us  [shards(): jnp.concatenate([padded(gain[None], 1), padded(norm[None], 7), padded(spi...]
    unnamed x1 -> x3, local copies, waits for them, and re-layouts: 1.87 us -> 1.45 us
where the time goes in v5:
time: 45 us; the launch traced here: 44.8 us
  Pallas kernels  42.5 us (94%)
  local copies, waits for them, and re-layouts  1.45 us (3%)
  other arithmetic  0.76 us (2%)
    pallas_call x1, Pallas kernels, shards(): pl.pallas_call(functools.partial(layer_kernel, sp, tp, list(inputs) + ['o...  42.5 us
    unnamed x3, local copies, waits for them, and re-layouts  1.45 us

profile of v5, /device:TPU:18, one launch (start us, length us, event | category | flops | bytes accessed | tf_op | source)
XLA Modules:
  0.0 44.8 jit_solution(4045937011629444031)
XLA Ops:
  0.0 0.8 %select_maximum_fusion.refs_1_ = f32[24,2048]{1,0:T(8,128)S(1)} fusion(f32[4,128]{1,0:T(4,128)} %param.25, f32[4,256]{1,0:T(4,128)} %bitcast.4, f32[1,64]{1,0:T(1,128)} %bitcast.5, f32[1,2048]{1,0:T(1,128)} %bitcast.3), kind=kLoop, calls=%fused_computation.4 | loop fusion | flops 638976 | bytes 211200 | tf_op jit(solution)/shard_map/concatenate | solution.py:623
  0.8 0.0 copy-start
  0.8 0.6 %copy-done = f32[4]{0:T(128)S(1)} copy-done((f32[4]{0:T(128)S(1)}, f32[4]{0:T(128)}, u32[]{:S(2)}) %copy-start) | copy-done | bytes 40
  1.4 42.5 %layer.1 = bf16[256,1024]{1,0:T(8,128)(2,1)S(1)} custom-call(bf16[256,1024]{1,0:T(8,128)(2,1)} %refs_0_.1, f32[24,2048]{1,0:T(8,128)S(1)} %select_maximum_fusion.refs_1_, bf16[2048,256]{1,0:T(8,128)(2,1)} %refs_2_.1, bf16[2048,256]{1,0:T(8,128)(2,1)} %refs_3_.1, bf16[2048,256]{1,0:T(8,128)(2,1)} %refs_4_.1, bf16[2048,512]{1,0:T(8,128)(2,1)} %refs_5_.1, ...), custom_call_target="tpu_custom_call" | custom-call | tf_op jit(solution)/shard_map/layer/pallas_call | solution.py:693
  44.0 0.8 %copy.17 = bf16[256,1024]{1,0:T(8,128)(2,1)} copy(bf16[256,1024]{1,0:T(8,128)(2,1)S(1)} %layer.1) | data formatting | bytes 1048576
Async XLA Ops:
  0.8 0.7 %copy-start = (f32[4]{0:T(128)S(1)}, f32[4]{0:T(128)}, u32[]{:S(2)}) copy-start(f32[4]{0:T(128)} %refs_9_.1) | copy-start | bytes 52

commit v6 on v5

--- a/solution.py
+++ b/solution.py
@@ -310,8 +310,8 @@
 
     for name in "rfi":
         project(name, last_rows)
+    wave_events(2, 0)
     wave_events(1, chunks - 2)
-    wave_events(2, 0)
     recur(1)
 
     def s_copy(off):

time: 45 us -> 45 us (level)
  no operation moved by 1% of the time
where the time goes in v6:
time: 45 us; the launch traced here: 44.8 us
  Pallas kernels  42.5 us (94%)
  local copies, waits for them, and re-layouts  1.45 us (3%)
  other arithmetic  0.76 us (2%)
    pallas_call x1, Pallas kernels, shards(): pl.pallas_call(functools.partial(layer_kernel, sp, tp, list(inputs) + ['o...  42.5 us
    unnamed x3, local copies, waits for them, and re-layouts  1.45 us

profile of v6, /device:TPU:18, one launch (start us, length us, event | category | flops | bytes accessed | tf_op | source)
XLA Modules:
  0.0 44.8 jit_solution(6019024132786268677)
XLA Ops:
  0.0 0.8 %select_maximum_fusion.refs_1_ = f32[24,2048]{1,0:T(8,128)S(1)} fusion(f32[4,128]{1,0:T(4,128)} %param.25, f32[4,256]{1,0:T(4,128)} %bitcast.4, f32[1,64]{1,0:T(1,128)} %bitcast.5, f32[1,2048]{1,0:T(1,128)} %bitcast.3), kind=kLoop, calls=%fused_computation.4 | loop fusion | flops 638976 | bytes 211200 | tf_op jit(solution)/shard_map/concatenate | solution.py:623
  0.8 0.0 copy-start
  0.8 0.6 %copy-done = f32[4]{0:T(128)S(1)} copy-done((f32[4]{0:T(128)S(1)}, f32[4]{0:T(128)}, u32[]{:S(2)}) %copy-start) | copy-done | bytes 40
  1.4 42.5 %layer.1 = bf16[256,1024]{1,0:T(8,128)(2,1)S(1)} custom-call(bf16[256,1024]{1,0:T(8,128)(2,1)} %refs_0_.1, f32[24,2048]{1,0:T(8,128)S(1)} %select_maximum_fusion.refs_1_, bf16[2048,256]{1,0:T(8,128)(2,1)} %refs_2_.1, bf16[2048,256]{1,0:T(8,128)(2,1)} %refs_3_.1, bf16[2048,256]{1,0:T(8,128)(2,1)} %refs_4_.1, bf16[2048,512]{1,0:T(8,128)(2,1)} %refs_5_.1, ...), custom_call_target="tpu_custom_call" | custom-call | tf_op jit(solution)/shard_map/layer/pallas_call | solution.py:693
  44.0 0.8 %copy.17 = bf16[256,1024]{1,0:T(8,128)(2,1)} copy(bf16[256,1024]{1,0:T(8,128)(2,1)S(1)} %layer.1) | data formatting | bytes 1048576
Async XLA Ops:
  0.8 0.7 %copy-start = (f32[4]{0:T(128)S(1)}, f32[4]{0:T(128)}, u32[]{:S(2)}) copy-start(f32[4]{0:T(128)} %refs_9_.1) | copy-start | bytes 52
